TPU v7x, 32 devices: a whole 2x2x4 slice. The times are simulated.
32 devices in a mesh: sp: 8 (over z, y), tp: 4 (over x, core).
Axes of the slice: x: 2, y: 2, z: 4, core: 2. Of those that a mesh axis runs over, the one named last changes fastest.
Arguments:
- residual: bfloat16 [4096, 2048], P(('sp', 'tp')), may hold values from -6 to 6
- query_proj: bfloat16 [4096, 2048], P('sp', 'tp'), may hold values from -12 to 12
- key_proj: bfloat16 [4096, 512], P('sp', 'tp'), may hold values from -12 to 12
- value_proj: bfloat16 [4096, 512], P('sp', 'tp'), may hold values from -6 to 6
- query_gain: float32 [128], replicated, may hold values from 0.4 to 4.5
- key_gain: float32 [128], replicated, may hold values from 0.4 to 4.5
- document_ids: int32 [4096], P('sp'), may hold values from 0 to 3, never falling along the last dimension, each value on 1 to 1537 neighbouring positions
- output_weight: bfloat16 [2048, 2048], replicated, may hold values from -0.125 to 0.125
- norm_gain: float32 [2048], replicated, may hold values from 0.1 to 1.9
- expert_ids: int32 [4096, 2], P(('sp', 'tp')), may hold values from 0 to 31, all different within a row; in each aligned block of 128 rows (0 to 127, 128 to 255, ...) at most 16 rows name the same one
- route_weights: float32 [4096, 2], P(('sp', 'tp')), may hold values from 0.2 to 1
- gate_weight: bfloat16 [32, 2048, 512], P(('sp', 'tp')), may hold values from -0.125 to 0.125
- up_weight: bfloat16 [32, 2048, 512], P(('sp', 'tp')), may hold values from -0.125 to 0.125
- down_weight: bfloat16 [32, 512, 2048], P(('sp', 'tp')), may hold values from -0.25 to 0.25
Outputs:
- updated: bfloat16 [4096, 2048], P(('sp', 'tp'))
Inputs may be any that keep to these rules, and one draw needn't show every extreme that they name: `document_ids`: document numbers never fall along the positions; each document has at most 1537 positions, and one has exactly 1537. `expert_ids`: each row names 2 different experts; within the rows of one device no expert is named more than 16 times, and in some device's rows an expert is named exactly 16 times.
All inputs are finite; a program needn't handle non-finite values.
Results may differ from a plain program's by a relative error of at most 0.017.
Values may be sent and summed in bfloat16 or wider, within the bound.
A program may use at most 128 MiB of HBM per device.

v0:
```python
import functools
import math

import jax
import jax.numpy as jnp
from jax import lax
from jax.experimental import pallas as pl
from jax.experimental.pallas import tpu as pltpu
from jax.sharding import PartitionSpec as P

HEAD = 128
GRID_W = 64
REACH = 3


norm_eps = 1e-06
rope_base = 10000.0
masked_low = -1e30
MESH = pl.DeviceIdType.MESH
DOC_KEY = 128.0
DOC_QUERY = 64.0
EXP2_SCALE = math.log2(math.e) / math.sqrt(HEAD)


def rotary_tables(first_row, length):
    freq_count = HEAD // 4
    inverse = 1.0 / rope_base ** (jnp.arange(freq_count, dtype=jnp.float32) / freq_count)
    position = first_row + jnp.arange(length, dtype=jnp.int32)
    grid_row = (position // GRID_W).astype(jnp.float32)
    grid_col = (position % GRID_W).astype(jnp.float32)
    angles = jnp.concatenate(
        [grid_row[:, None] * inverse[None, :], grid_col[:, None] * inverse[None, :]], axis=1
    )
    return (jnp.cos(angles), jnp.sin(angles))


def norm_rotate(projected, gains, cosine, sine_table):
    length = projected.shape[0]
    values_wide = projected.astype(jnp.float32).reshape(length, -1, HEAD)
    scaled = (
        values_wide
        * lax.rsqrt(jnp.mean(values_wide * values_wide, axis=-1, keepdims=True) + norm_eps)
        * gains
    )
    half_size = HEAD // 2
    first_half = scaled[..., :half_size]
    second_half = scaled[..., half_size:]
    cosine_rows = cosine[:, None, :]
    sine_rows = sine_table[:, None, :]
    turned = jnp.concatenate(
        [
            first_half * cosine_rows - second_half * sine_rows,
            first_half * sine_rows + second_half * cosine_rows,
        ],
        axis=-1,
    )
    return turned.reshape(length, -1).astype(jnp.bfloat16)


def attention_kernel(
    n_sp, n_tp, q_ref, k_ref, vt_ref, doc_ref, res_ref, gain_ref, wo_hbm,
    hid_ref, nrm_ref,
    wo_v, k_in, vt_in, doc_in, k_aug, m_s, l_s, acc_s, att_s, all_s,
    send, recv, t_send, t_recv, w_sem,
):
    sp = lax.axis_index("sp")
    tp = lax.axis_index("tp")
    heads = q_ref.shape[0]
    rows = res_ref.shape[0]
    width = att_s.shape[1]
    slots = 2 * REACH

    def distance(j):
        return (j // 2 + 1) * (1 - 2 * (j % 2))

    def inside(index):
        return jnp.logical_and(index >= 0, index < n_sp)

    wo_copy = pltpu.make_async_copy(wo_hbm, wo_v, w_sem)
    wo_copy.start()

    barrier = pltpu.get_barrier_semaphore()
    for j in range(slots):
        there = sp + distance(j)

        @pl.when(inside(there))
        def _():
            pl.semaphore_signal(barrier, inc=1, device_id=(there, tp), device_id_type=MESH)

    for k in range(1, n_tp):
        pl.semaphore_signal(
            barrier, inc=1, device_id=(sp, lax.rem(tp + k, n_tp)), device_id_type=MESH
        )
    beside = jnp.minimum(sp, REACH) + jnp.minimum(n_sp - 1 - sp, REACH)
    pl.semaphore_wait(barrier, n_tp - 1 + beside)

    def copies(j):
        there = (sp + distance(j), tp)
        return [
            pltpu.make_async_remote_copy(
                src_ref=one,
                dst_ref=into.at[j],
                send_sem=send.at[j, i],
                recv_sem=recv.at[j, i],
                device_id=there,
                device_id_type=MESH,
            )
            for i, (one, into) in enumerate(((k_ref, k_in), (vt_ref, vt_in), (doc_ref, doc_in)))
        ]

    for j in range(slots):

        @pl.when(inside(sp + distance(j)))
        def _():
            for copy in copies(j):
                copy.start()

    def take(keys, values_t, docs, first):
        length = keys.shape[0]
        doc_col = jnp.broadcast_to(docs[0:1, :], (HEAD, length)).T
        lanes = lax.broadcasted_iota(jnp.int32, (length, HEAD), 1).astype(jnp.float32)
        k_aug[:, :HEAD] = keys[...]
        k_aug[:, HEAD:] = jnp.where(doc_col == lanes, DOC_KEY, 0.0).astype(jnp.bfloat16)
        for h in range(heads):
            s = jnp.dot(k_aug[...], q_ref[h], preferred_element_type=jnp.float32)
            top = jnp.max(s, axis=0, keepdims=True)
            if not first:
                top = jnp.maximum(m_s[h], top)
            e = jnp.exp2((s - top) * EXP2_SCALE)
            den = jnp.sum(e, axis=0, keepdims=True)
            part = jnp.dot(
                values_t[...], e.astype(jnp.bfloat16), preferred_element_type=jnp.float32
            )
            if first:
                l_s[h] = den
                acc_s[h] = part
            else:
                old = jnp.exp2((m_s[h] - top) * EXP2_SCALE)
                l_s[h] = l_s[h] * old + den
                acc_s[h] = acc_s[h] * old + part
            m_s[h] = top

    take(k_ref, vt_ref, doc_ref, True)

    def step(j, carry):
        @pl.when(inside(sp - distance(j)))
        def _():
            for copy in copies(j):
                copy.wait_recv()
            take(k_in.at[j], vt_in.at[j], doc_in.at[j], False)

        return carry

    lax.fori_loop(0, slots, step, 0)

    for h in range(heads):
        out = acc_s[h] / l_s[h]
        att_s[:, h * HEAD : (h + 1) * HEAD] = out.T.astype(jnp.bfloat16)

    def exchange(k):
        there = lax.rem(tp + k, n_tp)
        return pltpu.make_async_remote_copy(
            src_ref=att_s.at[pl.ds(pl.multiple_of(there * rows, rows), rows), :],
            dst_ref=all_s.at[tp],
            send_sem=t_send.at[k],
            recv_sem=t_recv.at[k],
            device_id=(sp, there),
            device_id_type=MESH,
        )

    for k in range(n_tp - 1, 0, -1):
        exchange(k).start()
    wo_copy.wait()

    def weight_rows(i):
        return wo_v[pl.ds(pl.multiple_of(i * width, width), width), :]

    projected = jnp.dot(
        att_s[pl.ds(pl.multiple_of(tp * rows, rows), rows), :],
        weight_rows(tp),
        preferred_element_type=jnp.float32,
    )
    for k in range(1, n_tp):
        exchange(k).wait_recv()
        source = lax.rem(tp - k + n_tp, n_tp)
        projected += jnp.dot(
            all_s[source], weight_rows(source), preferred_element_type=jnp.float32
        )
    hidden = (res_ref[...].astype(jnp.float32) + projected).astype(jnp.bfloat16)
    hid_ref[...] = hidden
    wide = hidden.astype(jnp.float32)
    mean = jnp.mean(wide * wide, axis=-1, keepdims=True)
    nrm_ref[...] = (wide * lax.rsqrt(mean + norm_eps) * gain_ref[...]).astype(jnp.bfloat16)

    for j in range(slots):

        @pl.when(inside(sp + distance(j)))
        def _():
            for copy in copies(j):
                copy.wait_send()

    for k in range(1, n_tp):
        exchange(k).wait_send()


def attend(q_aug, key_norm, value_t, doc_rows, residual, norm_gain, output_weight):
    n_sp, n_tp = lax.axis_size("sp"), lax.axis_size("tp")
    heads, deep, length = q_aug.shape
    rows, model = residual.shape
    vmem = pl.BlockSpec(memory_space=pltpu.VMEM)
    slots = 2 * REACH
    return pl.pallas_call(
        functools.partial(attention_kernel, n_sp, n_tp),
        out_shape=[jax.ShapeDtypeStruct((rows, model), jnp.bfloat16)] * 2,
        in_specs=[vmem] * 6 + [pl.BlockSpec(memory_space=pl.ANY)],
        out_specs=[vmem] * 2,
        scratch_shapes=[
            pltpu.VMEM(output_weight.shape, jnp.bfloat16),
            pltpu.VMEM((slots,) + key_norm.shape, jnp.bfloat16),
            pltpu.VMEM((slots,) + value_t.shape, jnp.bfloat16),
            pltpu.VMEM((slots,) + doc_rows.shape, jnp.float32),
            pltpu.VMEM((length, deep), jnp.bfloat16),
            pltpu.VMEM((heads, 1, length), jnp.float32),
            pltpu.VMEM((heads, 1, length), jnp.float32),
            pltpu.VMEM((heads, HEAD, length), jnp.float32),
            pltpu.VMEM((length, heads * HEAD), jnp.bfloat16),
            pltpu.VMEM((n_tp, rows, heads * HEAD), jnp.bfloat16),
            pltpu.SemaphoreType.DMA((slots, 3)),
            pltpu.SemaphoreType.DMA((slots, 3)),
            pltpu.SemaphoreType.DMA((n_tp,)),
            pltpu.SemaphoreType.DMA((n_tp,)),
            pltpu.SemaphoreType.DMA(()),
        ],
        compiler_params=pltpu.CompilerParams(
            collective_id=1, has_side_effects=True, vmem_limit_bytes=48 * 1024 * 1024
        ),
    )(q_aug, key_norm, value_t, doc_rows, residual, norm_gain.reshape(1, -1), output_weight)


def expert_kernel(
    n_tp, capacity, out_ref, high_ref, low_ref, hid_ref, gate_hbm, up_hbm, down_hbm,
    new_ref,
    gate_v, up_v, down_v, arrived, answer, returned,
    d_send, d_recv, r_send, r_recv, w_sem,
):
    me = lax.axis_index("sp") * n_tp + lax.axis_index("tp")
    devices = out_ref.shape[0] // capacity
    rows = hid_ref.shape[0]
    members = rows // capacity
    groups = devices // members
    my_group = lax.div(me, members)
    my_place = lax.rem(me, members)

    loads = [
        pltpu.make_async_copy(source.at[0], into, w_sem.at[i])
        for i, (source, into) in enumerate(
            ((gate_hbm, gate_v), (up_hbm, up_v), (down_hbm, down_v))
        )
    ]
    for load in loads:
        load.start()

    def place(device):
        return (lax.div(device, n_tp), lax.rem(device, n_tp))

    def slots(device):
        return pl.ds(pl.multiple_of(device * capacity, capacity), capacity)

    barrier = pltpu.get_barrier_semaphore()

    def greet(i, carry):
        there = lax.rem(me + i, devices)
        pl.semaphore_signal(barrier, inc=1, device_id=place(there), device_id_type=MESH)
        return carry

    lax.fori_loop(1, devices, greet, 0)
    pl.semaphore_wait(barrier, devices - 1)

    def dispatch(device, landing):
        return pltpu.make_async_remote_copy(
            src_ref=out_ref.at[slots(device)],
            dst_ref=arrived.at[slots(landing)],
            send_sem=d_send.at[device],
            recv_sem=d_recv.at[landing],
            device_id=place(device),
            device_id_type=MESH,
        )

    def give_back(device, landing):
        return pltpu.make_async_remote_copy(
            src_ref=answer.at[slots(device)],
            dst_ref=returned.at[slots(landing)],
            send_sem=r_send.at[device],
            recv_sem=r_recv.at[landing],
            device_id=place(device),
            device_id_type=MESH,
        )

    def each(group, skip_self, act):
        def one(i, carry):
            act(group * members + lax.rem(my_place + i, members))
            return carry

        lax.fori_loop(1 if skip_self else 0, members, one, 0)

    def group_at(step):
        return lax.rem(my_group + step + groups, groups)

    def group_rows(group):
        return pl.ds(pl.multiple_of(group * rows, rows), rows)

    for c in range(groups):
        each(group_at(c), c == 0, lambda device: dispatch(device, me).start())
    arrived[slots(me), :] = out_ref[slots(me), :]
    for load in loads:
        load.wait()

    for c in range(groups):
        group = group_at(-c)
        each(group, c == 0, lambda device: dispatch(device, device).wait_recv())
        x = arrived[group_rows(group), :]
        gate_part = jnp.dot(x, gate_v[...], preferred_element_type=jnp.float32)
        up_part = jnp.dot(x, up_v[...], preferred_element_type=jnp.float32)
        activity = (jax.nn.silu(gate_part) * up_part).astype(jnp.bfloat16)
        answer[group_rows(group), :] = jnp.dot(
            activity, down_v[...], preferred_element_type=jnp.float32
        ).astype(jnp.bfloat16)
        each(group, c == 0, lambda device: give_back(device, me).start())
    returned[slots(me), :] = answer[slots(me), :]

    total = hid_ref[...].astype(jnp.float32)
    for c in range(groups):
        group = group_at(c)
        each(group, c == 0, lambda device: give_back(device, device).wait_recv())
        back = returned[group_rows(group), :]
        lanes = group_rows(group)
        total += jnp.dot(high_ref[:, lanes], back, preferred_element_type=jnp.float32)
        total += jnp.dot(low_ref[:, lanes], back, preferred_element_type=jnp.float32)
    new_ref[...] = total.astype(jnp.bfloat16)

    for c in range(groups):
        each(group_at(c), c == 0, lambda device: dispatch(device, me).wait_send())
        each(group_at(c), c == 0, lambda device: give_back(device, me).wait_send())


def run_experts(outgoing, high, low, hidden, gate_weight, up_weight, down_weight, capacity):
    n_tp = lax.axis_size("tp")
    devices = outgoing.shape[0] // capacity
    vmem = pl.BlockSpec(memory_space=pltpu.VMEM)
    anywhere = pl.BlockSpec(memory_space=pl.ANY)
    buffer = pltpu.VMEM(outgoing.shape, jnp.bfloat16)
    return pl.pallas_call(
        functools.partial(expert_kernel, n_tp, capacity),
        out_shape=jax.ShapeDtypeStruct(hidden.shape, jnp.bfloat16),
        in_specs=[vmem] * 4 + [anywhere] * 3,
        out_specs=vmem,
        scratch_shapes=[
            pltpu.VMEM(gate_weight.shape[1:], jnp.bfloat16),
            pltpu.VMEM(up_weight.shape[1:], jnp.bfloat16),
            pltpu.VMEM(down_weight.shape[1:], jnp.bfloat16),
            buffer,
            buffer,
            buffer,
            pltpu.SemaphoreType.DMA((devices,)),
            pltpu.SemaphoreType.DMA((devices,)),
            pltpu.SemaphoreType.DMA((devices,)),
            pltpu.SemaphoreType.DMA((devices,)),
            pltpu.SemaphoreType.DMA((3,)),
        ],
        compiler_params=pltpu.CompilerParams(
            collective_id=2, has_side_effects=True, vmem_limit_bytes=40 * 1024 * 1024
        ),
    )(outgoing, high, low, hidden, gate_weight, up_weight, down_weight)


def on_device(
    residual,
    query_proj,
    key_proj,
    value_proj,
    query_gain,
    key_gain,
    document_ids,
    output_weight,
    norm_gain,
    expert_ids,
    route_weights,
    gate_weight,
    up_weight,
    down_weight,
):
    rows_here = query_proj.shape[0]
    cosine, sine_table = rotary_tables(lax.axis_index("sp") * rows_here, rows_here)
    query_norm = norm_rotate(query_proj, query_gain, cosine, sine_table)
    key_norm = norm_rotate(key_proj, key_gain, cosine, sine_table)
    heads = query_proj.shape[1] // HEAD
    docs = document_ids.astype(jnp.float32)
    query_t = jnp.transpose(query_norm.reshape(rows_here, heads, HEAD), (1, 2, 0))
    query_doc = jnp.where(
        docs[None, :] == jnp.arange(HEAD, dtype=jnp.float32)[:, None], DOC_QUERY, 0.0
    ).astype(jnp.bfloat16)
    q_aug = jnp.concatenate(
        [query_t, jnp.broadcast_to(query_doc[None], (heads, HEAD, rows_here))], axis=1
    )
    doc_rows = jnp.broadcast_to(docs[None, :], (8, rows_here))
    hidden, normed = attend(
        q_aug, key_norm, value_proj.T, doc_rows, residual, norm_gain, output_weight
    )
    token_rows = residual.shape[0]
    top_count = expert_ids.shape[1]
    experts_all = lax.axis_size("sp") * lax.axis_size("tp")
    capacity = max(2, 2 * token_rows * top_count // experts_all)
    flat_ids = expert_ids.reshape(-1)
    order = jnp.arange(flat_ids.shape[0], dtype=jnp.int32)
    earlier = jnp.logical_and(
        flat_ids[:, None] == flat_ids[None, :], order[None, :] < order[:, None]
    )
    arrival = jnp.sum(earlier.astype(jnp.int32), axis=1)
    slot_index = flat_ids * capacity + arrival
    slot_grid = slot_index.reshape(token_rows, top_count)
    placing = jnp.sum(
        (
            jnp.arange(experts_all * capacity, dtype=jnp.int32)[:, None, None] == slot_grid[None]
        ).astype(jnp.float32),
        axis=2,
    ).astype(jnp.bfloat16)
    outgoing = jnp.dot(placing, normed, preferred_element_type=jnp.float32).astype(jnp.bfloat16)
    spread = jnp.sum(
        jnp.where(
            jnp.arange(experts_all * capacity, dtype=jnp.int32)[None, None, :]
            == slot_grid[:, :, None],
            route_weights[:, :, None],
            0.0,
        ),
        axis=1,
    )
    high = spread.astype(jnp.bfloat16)
    low = (spread - high.astype(jnp.float32)).astype(jnp.bfloat16)
    if capacity % 16 == 0 and token_rows % capacity == 0 and experts_all % (token_rows // capacity) == 0:
        return run_experts(
            outgoing, high, low, hidden, gate_weight, up_weight, down_weight, capacity
        )
    outgoing = outgoing.reshape(experts_all, capacity, normed.shape[1])
    arrived = lax.all_to_all(outgoing, ("sp", "tp"), split_axis=0, concat_axis=0, tiled=True)
    sources, slots, width = arrived.shape
    flat_rows = arrived.reshape(sources * slots, width)
    gate_part = jnp.dot(flat_rows, gate_weight[0], preferred_element_type=jnp.float32)
    up_part = jnp.dot(flat_rows, up_weight[0], preferred_element_type=jnp.float32)
    activity = (jax.nn.silu(gate_part) * up_part).astype(jnp.bfloat16)
    expert_out = jnp.dot(activity, down_weight[0], preferred_element_type=jnp.float32).astype(
        jnp.bfloat16
    )
    returned = lax.all_to_all(
        expert_out.reshape(sources, slots, width),
        ("sp", "tp"),
        split_axis=0,
        concat_axis=0,
        tiled=True,
    )
    rows_back = returned.reshape(experts_all * capacity, -1)
    combined = jnp.dot(high, rows_back, preferred_element_type=jnp.float32) + jnp.dot(
        low, rows_back, preferred_element_type=jnp.float32
    )
    return (hidden.astype(jnp.float32) + combined).astype(jnp.bfloat16)


def solution(mesh):
    in_specs = (
        P(("sp", "tp"), None),
        P("sp", "tp"),
        P("sp", "tp"),
        P("sp", "tp"),
        P(),
        P(),
        P("sp"),
        P(),
        P(),
        P(("sp", "tp"), None),
        P(("sp", "tp"), None),
        P(("sp", "tp"), None, None),
        P(("sp", "tp"), None, None),
        P(("sp", "tp"), None, None),
    )
    out_specs = P(("sp", "tp"), None)
    return jax.shard_map(
        on_device, mesh=mesh, in_specs=in_specs, out_specs=out_specs, check_vma=False
    )
```

profile of v0, /device:TPU:0, one launch (start us, length us, event | category | flops | bytes accessed | tf_op | source)
XLA Modules:
  0.0 164.3 jit_solution(6326406131868241553)
XLA Ops:
  0.0 0.2 fusion.9
  0.2 0.0 copy-start.11
  0.2 1.1 fusion.8
  1.4 0.1 copy.42
  1.5 0.1 copy.43
  1.6 0.0 copy-done.5
  1.6 0.2 copy.41
  1.8 0.1 multiply_reduce_fusion
  2.0 0.0 copy-done.11
  2.0 0.0 copy-start.9
  2.0 0.2 multiply_multiply_fusion
  2.2 0.2 subtract_convert_fusion
  2.4 0.0 copy-start.6
  2.4 0.0 copy-start.12
  2.5 0.2 copy-done.9
  2.8 0.0 copy-start.7
  2.8 0.0 copy-start.3
  2.8 0.0 copy-start.4
  2.8 0.1 pad_maximum_fusion.q_ref
  2.9 0.4 copy-done.6
  3.3 0.1 fusion
  3.5 0.0 copy-done.12
  3.5 0.1 fusion.2
  3.6 1.2 subtract_convert_fusion.2
  4.8 0.1 maximum_bitcast_fusion.1.k_ref
  4.9 0.0 copy-done.7
  5.0 0.1 copy.44
  5.1 0.0 copy-done.3
  5.1 0.0 copy-done.4
  5.1 0.0 copy-start.8
  5.1 31.2 %shard_map.136 = (bf16[128,2048]{1,0:T(8,128)(2,1)S(1)}, bf16[128,2048]{1,0:T(8,128)(2,1)S(1)}) custom-call(bf16[4,256,512]{2,1,0:T(8,128)(2,1)S(1)} %pad_maximum_fusion.q_ref, bf16[512,128]{1,0:T(8,128)(2,1)S(1)} %maximum_bitcast_fusion.1.k_ref, bf16[128,512]{1,0:T(8,128)(2,1)S(1)} %bitcast.17, f32[8,512]{1,0:T(8,128)S(1)} %broadcast_in_dim.23.doc_ref, ...), custom_call_target="tpu_custom_call" | custom-call | tf_op jit(solution)/shard_map/pallas_call | solution.py:212
  36.4 0.0 copy-start.10
  36.4 0.0 copy-start
  36.4 0.0 copy-done.8
  36.4 0.1 copy.39
  36.5 0.1 eq.61
  36.6 0.2 convert_reduce_fusion.1
  36.8 0.1 reduce_sum.48
  37.0 0.1 copy.40
  37.0 0.1 convert_reduce_fusion
  37.1 0.7 convolution_convert_fusion.out_ref
  37.8 0.0 copy-done.10
  37.9 0.1 select_reduce_fusion
  38.0 0.0 copy-start.1
  38.1 1.6 copy-done.1
  39.6 1.6 copy-done.2
  41.2 122.3 %shard_map.137 = bf16[128,2048]{1,0:T(8,128)(2,1)S(1)} custom-call(bf16[512,2048]{1,0:T(8,128)(2,1)S(1)} %convolution_convert_fusion.out_ref, bf16[128,512]{1,0:T(8,128)(2,1)S(1)} %get-tuple-element.10.high_ref, bf16[128,512]{1,0:T(8,128)(2,1)S(1)} %get-tuple-element.9.low_ref, bf16[128,2048]{1,0:T(8,128)(2,1)S(1)} %get-tuple-element.8.hid_ref, ...), custom_call_target="tpu_custom_call" | custom-call | tf_op jit(solution)/shard_map/pallas_call | solution.py:352
  163.6 0.8 copy.46
  (14 shorter events, 0.2 us)
Async XLA Ops:
  0.0 1.6 copy-start.5
  0.2 1.8 %copy-start.11 = (f32[128]{0:T(128)S(1)}, f32[128]{0:T(128)}, u32[]{:S(2)}) copy-start(f32[128]{0:T(128)} %param.18) | copy-start | bytes 1540
  2.0 0.7 copy-start.9
  2.4 0.9 copy-start.6
  2.4 1.1 copy-start.12
  2.8 2.2 %copy-start.7 = (bf16[512,128]{1,0:T(8,128)(2,1)S(1)}, bf16[512,128]{1,0:T(8,128)(2,1)}, u32[]{:S(2)}) copy-start(bf16[512,128]{1,0:T(8,128)(2,1)} %param.17) | copy-start | bytes 393220
  2.8 2.3 %copy-start.3 = (bf16[128,2048]{1,0:T(8,128)(2,1)S(1)}, bf16[128,2048]{1,0:T(8,128)(2,1)}, u32[]{:S(2)}) copy-start(bf16[128,2048]{1,0:T(8,128)(2,1)} %res_ref.1) | copy-start | bytes 1572868
  2.8 2.3 %copy-start.4 = (f32[2048]{0:T(1024)S(1)}, f32[2048]{0:T(1024)}, u32[]{:S(2)}) copy-start(f32[2048]{0:T(1024)} %param.22) | copy-start | bytes 24580
  5.1 31.3 %copy-start.8 = (s32[128,2]{0,1:T(2,128)S(1)}, s32[128,2]{0,1:T(2,128)}, u32[]{:S(2)}) copy-start(s32[128,2]{0,1:T(2,128)} %param.23) | copy-start | bytes 3076
  36.4 1.5 copy-start.10
  36.4 1.7 %copy-start = (bf16[1,2048,512]{2,1,0:T(8,128)(2,1)S(1)}, bf16[1,2048,512]{2,1,0:T(8,128)(2,1)}, u32[]{:S(2)}) copy-start(bf16[1,2048,512]{2,1,0:T(8,128)(2,1)} %gate_hbm.1) | copy-start | bytes 6291460
  38.0 1.6 copy-start.1
  39.6 1.6 copy-start.2
where the time goes:
time: 165 us; the launch traced here: 164 us
  Pallas kernels  154 us (93%)
  local copies, waits for them, and re-layouts  5.71 us (3%)
  other arithmetic  4.03 us (2%)
    pallas_call x1, Pallas kernels, run_experts(): pl.pallas_call(functools.partial(expert_kernel, n_tp, capacity), out_shap...  122 us
    pallas_call x1, Pallas kernels, attend(): pl.pallas_call(functools.partial(attention_kernel, n_sp, n_tp), out_shape...  31.2 us
    unnamed x29, local copies, waits for them, and re-layouts  4.89 us

commit v1 on v0

--- a/solution.py
+++ b/solution.py
@@ -19,6 +19,7 @@
 MESH = pl.DeviceIdType.MESH
 DOC_KEY = 128.0
 DOC_QUERY = 64.0
+PIECES = 2
 EXP2_SCALE = math.log2(math.e) / math.sqrt(HEAD)
 
 
@@ -238,18 +239,20 @@
 
 
 def expert_kernel(
-    n_tp, capacity, out_ref, high_ref, low_ref, hid_ref, gate_hbm, up_hbm, down_hbm,
+    n_sp, n_tp, capacity, top_count,
+    nrm_ref, meta_ref, hid_ref, gate_hbm, up_hbm, down_hbm,
     new_ref,
-    gate_v, up_v, down_v, arrived, answer, returned,
-    d_send, d_recv, r_send, r_recv, w_sem,
+    gate_v, up_v, down_v, metas, blocks, picked, arrived, answer, returned, spread,
+    m_send, m_recv, z_send, z_recv, d_send, d_recv, r_send, r_recv, w_sem,
 ):
-    me = lax.axis_index("sp") * n_tp + lax.axis_index("tp")
-    devices = out_ref.shape[0] // capacity
+    devices = n_sp * n_tp
     rows = hid_ref.shape[0]
     members = rows // capacity
     groups = devices // members
-    my_group = lax.div(me, members)
-    my_place = lax.rem(me, members)
+    piece = rows // PIECES
+    me = lax.axis_index("sp") * n_tp + lax.axis_index("tp")
+    plane = lax.div(me, members)
+    pos = lax.rem(me, members)
 
     loads = [
         pltpu.make_async_copy(source.at[0], into, w_sem.at[i])
@@ -263,8 +266,11 @@
     def place(device):
         return (lax.div(device, n_tp), lax.rem(device, n_tp))
 
-    def slots(device):
-        return pl.ds(pl.multiple_of(device * capacity, capacity), capacity)
+    def slots(index):
+        return pl.ds(pl.multiple_of(index * capacity, capacity), capacity)
+
+    def inside(block):
+        return jnp.logical_and(block >= 0, block < groups)
 
     barrier = pltpu.get_barrier_semaphore()
 
@@ -276,101 +282,238 @@
     lax.fori_loop(1, devices, greet, 0)
     pl.semaphore_wait(barrier, devices - 1)
 
-    def dispatch(device, landing):
+    def tell(i, block):
         return pltpu.make_async_remote_copy(
-            src_ref=out_ref.at[slots(device)],
-            dst_ref=arrived.at[slots(landing)],
-            send_sem=d_send.at[device],
-            recv_sem=d_recv.at[landing],
-            device_id=place(device),
+            src_ref=meta_ref,
+            dst_ref=metas.at[block],
+            send_sem=m_send.at[i],
+            recv_sem=m_recv.at[block],
+            device_id=place(lax.rem(plane + i, groups) * members + pos),
             device_id_type=MESH,
         )
 
-    def give_back(device, landing):
+    def pass_on(source, block, way, c):
+        part = pl.ds(c * piece, piece)
         return pltpu.make_async_remote_copy(
-            src_ref=answer.at[slots(device)],
+            src_ref=source.at[part],
+            dst_ref=blocks.at[block, part],
+            send_sem=z_send.at[way, block, c],
+            recv_sem=z_recv.at[block, c],
+            device_id=place(me + (2 * way - 1) * members),
+            device_id_type=MESH,
+        )
+
+    def dispatch(block, peer, landing):
+        return pltpu.make_async_remote_copy(
+            src_ref=picked.at[block, slots(peer)],
+            dst_ref=arrived.at[block, slots(landing)],
+            send_sem=d_send.at[block, peer],
+            recv_sem=d_recv.at[block, landing],
+            device_id=place(plane * members + peer),
+            device_id_type=MESH,
+        )
+
+    def give_back(block, member, landing):
+        return pltpu.make_async_remote_copy(
+            src_ref=answer.at[block, slots(member)],
             dst_ref=returned.at[slots(landing)],
-            send_sem=r_send.at[device],
+            send_sem=r_send.at[block, member],
             recv_sem=r_recv.at[landing],
-            device_id=place(device),
+            device_id=place(block * members + member),
             device_id_type=MESH,
         )
 
-    def each(group, skip_self, act):
+    def others(act, first=1):
         def one(i, carry):
-            act(group * members + lax.rem(my_place + i, members))
+            act(lax.rem(pos + i, members))
             return carry
 
-        lax.fori_loop(1 if skip_self else 0, members, one, 0)
-
-    def group_at(step):
-        return lax.rem(my_group + step + groups, groups)
-
-    def group_rows(group):
-        return pl.ds(pl.multiple_of(group * rows, rows), rows)
-
-    for c in range(groups):
-        each(group_at(c), c == 0, lambda device: dispatch(device, me).start())
-    arrived[slots(me), :] = out_ref[slots(me), :]
-    for load in loads:
-        load.wait()
-
-    for c in range(groups):
-        group = group_at(-c)
-        each(group, c == 0, lambda device: dispatch(device, device).wait_recv())
-        x = arrived[group_rows(group), :]
+        lax.fori_loop(first, members, one, 0)
+
+    for i in range(1, groups):
+        tell(i, plane).start()
+    for way in range(2):
+
+        @pl.when(inside(plane + 2 * way - 1))
+        def _():
+            for c in range(PIECES):
+                pass_on(nrm_ref, plane, way, c).start()
+
+    def slot_rows(meta):
+        experts = lax.broadcasted_iota(jnp.int32, (devices, rows), 0).astype(jnp.float32)
+        hits = [experts == meta[k : k + 1, :] for k in range(top_count)]
+        named = sum(hit.astype(jnp.float32) for hit in hits)
+        ahead = (
+            lax.broadcasted_iota(jnp.int32, (rows, rows), 0)
+            < lax.broadcasted_iota(jnp.int32, (rows, rows), 1)
+        )
+        before = jnp.dot(
+            named.astype(jnp.bfloat16),
+            ahead.astype(jnp.float32).astype(jnp.bfloat16),
+            preferred_element_type=jnp.float32,
+        )
+        return [
+            meta[k : k + 1, :] * capacity
+            + jnp.sum(jnp.where(hits[k], before, 0.0), axis=0, keepdims=True)
+            for k in range(top_count)
+        ]
+
+    def slot_numbers(group):
+        return (
+            lax.broadcasted_iota(jnp.int32, (rows, rows), 0) + group * rows
+        ).astype(jnp.float32)
+
+    def gather(source, meta, block):
+        numbers = slot_numbers(plane)
+        choice = sum((numbers == row).astype(jnp.float32) for row in slot_rows(meta))
+        picked[block] = jnp.dot(
+            choice.astype(jnp.bfloat16), source[...], preferred_element_type=jnp.float32
+        ).astype(jnp.bfloat16)
+        others(lambda peer: dispatch(block, peer, pos).start())
+        arrived[block, slots(pos), :] = picked[block, slots(pos), :]
+
+    def expert(block):
+        others(lambda peer: dispatch(block, peer, peer).wait_recv())
+        x = arrived[block]
         gate_part = jnp.dot(x, gate_v[...], preferred_element_type=jnp.float32)
         up_part = jnp.dot(x, up_v[...], preferred_element_type=jnp.float32)
         activity = (jax.nn.silu(gate_part) * up_part).astype(jnp.bfloat16)
-        answer[group_rows(group), :] = jnp.dot(
+        answer[block] = jnp.dot(
             activity, down_v[...], preferred_element_type=jnp.float32
         ).astype(jnp.bfloat16)
-        each(group, c == 0, lambda device: give_back(device, me).start())
-    returned[slots(me), :] = answer[slots(me), :]
+
+    def both_ways(distance, act):
+        def one(way, carry):
+            block = plane - (2 * way - 1) * distance
+
+            @pl.when(inside(block))
+            def _():
+                act(block, way)
+
+            return carry
+
+        lax.fori_loop(0, 2, one, 0)
+
+    gather(nrm_ref, meta_ref[...], plane)
+    own_slots = slot_rows(meta_ref[...])
+    for g in range(groups):
+        numbers = slot_numbers(g)
+        weights = sum(
+            jnp.where(numbers == own_slots[k], meta_ref[top_count + k : top_count + k + 1, :], 0.0)
+            for k in range(top_count)
+        ).T
+        high = weights.astype(jnp.bfloat16)
+        spread[g, 0] = high
+        spread[g, 1] = (weights - high.astype(jnp.float32)).astype(jnp.bfloat16)
+    for load in loads:
+        load.wait()
+
+    def receive(block, way, c):
+        pass_on(nrm_ref, block, way, c).wait_recv()
+
+        @pl.when(inside(plane + 2 * way - 1))
+        def _():
+            pass_on(blocks.at[block], block, way, c).start()
+
+    def collect(block, way):
+        tell(1, block).wait_recv()
+        gather(blocks.at[block], metas[block], block)
+
+    def serve(block, way):
+        expert(block)
+        others(lambda member: give_back(block, member, me).start(), 0)
+
+    for distance in range(1, groups):
+        for c in range(PIECES):
+            if c == PIECES - 1:
+                if distance == 1:
+                    expert(plane)
+                    others(lambda member: give_back(plane, member, me).start())
+                    returned[slots(me), :] = answer[plane, slots(pos), :]
+                else:
+                    both_ways(distance - 1, serve)
+            both_ways(distance, functools.partial(receive, c=c))
+        both_ways(distance, collect)
+    both_ways(groups - 1, serve)
 
     total = hid_ref[...].astype(jnp.float32)
-    for c in range(groups):
-        group = group_at(c)
-        each(group, c == 0, lambda device: give_back(device, device).wait_recv())
-        back = returned[group_rows(group), :]
-        lanes = group_rows(group)
-        total += jnp.dot(high_ref[:, lanes], back, preferred_element_type=jnp.float32)
-        total += jnp.dot(low_ref[:, lanes], back, preferred_element_type=jnp.float32)
+
+    def combine(group):
+        back = returned[pl.ds(pl.multiple_of(group * rows, rows), rows), :]
+        part = jnp.dot(spread[group, 0], back, preferred_element_type=jnp.float32)
+        return part + jnp.dot(spread[group, 1], back, preferred_element_type=jnp.float32)
+
+    for i in range(groups):
+        group = lax.rem(plane + i, groups)
+        home = group * members
+        others(
+            lambda member: give_back(plane, member, home + member).wait_recv(), 1 if i == 0 else 0
+        )
+        total += combine(group)
     new_ref[...] = total.astype(jnp.bfloat16)
 
-    for c in range(groups):
-        each(group_at(c), c == 0, lambda device: dispatch(device, me).wait_send())
-        each(group_at(c), c == 0, lambda device: give_back(device, me).wait_send())
-
-
-def run_experts(outgoing, high, low, hidden, gate_weight, up_weight, down_weight, capacity):
-    n_tp = lax.axis_size("tp")
-    devices = outgoing.shape[0] // capacity
+    for i in range(1, groups):
+        tell(i, plane).wait_send()
+    for way in range(2):
+
+        @pl.when(inside(plane + 2 * way - 1))
+        def _():
+            for c in range(PIECES):
+                pass_on(nrm_ref, plane, way, c).wait_send()
+
+    def sent(block, way):
+        @pl.when(inside(plane + 2 * way - 1))
+        def _():
+            for c in range(PIECES):
+                pass_on(nrm_ref, block, way, c).wait_send()
+
+        others(lambda peer: dispatch(block, peer, pos).wait_send())
+        others(lambda member: give_back(block, member, me).wait_send(), 0)
+
+    others(lambda peer: dispatch(plane, peer, pos).wait_send())
+    others(lambda member: give_back(plane, member, me).wait_send())
+    for distance in range(1, groups):
+        both_ways(distance, sent)
+
+
+def run_experts(normed, meta, hidden, gate_weight, up_weight, down_weight, capacity, top_count):
+    n_sp, n_tp = lax.axis_size("sp"), lax.axis_size("tp")
+    rows, model = hidden.shape
+    members = rows // capacity
+    groups = n_sp * n_tp // members
     vmem = pl.BlockSpec(memory_space=pltpu.VMEM)
     anywhere = pl.BlockSpec(memory_space=pl.ANY)
-    buffer = pltpu.VMEM(outgoing.shape, jnp.bfloat16)
+    buffer = pltpu.VMEM((groups, rows, model), jnp.bfloat16)
     return pl.pallas_call(
-        functools.partial(expert_kernel, n_tp, capacity),
+        functools.partial(expert_kernel, n_sp, n_tp, capacity, top_count),
         out_shape=jax.ShapeDtypeStruct(hidden.shape, jnp.bfloat16),
-        in_specs=[vmem] * 4 + [anywhere] * 3,
+        in_specs=[vmem] * 3 + [anywhere] * 3,
         out_specs=vmem,
         scratch_shapes=[
             pltpu.VMEM(gate_weight.shape[1:], jnp.bfloat16),
             pltpu.VMEM(up_weight.shape[1:], jnp.bfloat16),
             pltpu.VMEM(down_weight.shape[1:], jnp.bfloat16),
+            pltpu.VMEM((groups,) + meta.shape, jnp.float32),
             buffer,
             buffer,
             buffer,
-            pltpu.SemaphoreType.DMA((devices,)),
-            pltpu.SemaphoreType.DMA((devices,)),
-            pltpu.SemaphoreType.DMA((devices,)),
-            pltpu.SemaphoreType.DMA((devices,)),
+            buffer,
+            pltpu.VMEM((groups * rows, model), jnp.bfloat16),
+            pltpu.VMEM((groups, 2, rows, rows), jnp.bfloat16),
+            pltpu.SemaphoreType.DMA((groups,)),
+            pltpu.SemaphoreType.DMA((groups,)),
+            pltpu.SemaphoreType.DMA((2, groups, PIECES)),
+            pltpu.SemaphoreType.DMA((groups, PIECES)),
+            pltpu.SemaphoreType.DMA((groups, members)),
+            pltpu.SemaphoreType.DMA((groups, members)),
+            pltpu.SemaphoreType.DMA((groups, members)),
+            pltpu.SemaphoreType.DMA((n_sp * n_tp,)),
             pltpu.SemaphoreType.DMA((3,)),
         ],
         compiler_params=pltpu.CompilerParams(
             collective_id=2, has_side_effects=True, vmem_limit_bytes=40 * 1024 * 1024
         ),
-    )(outgoing, high, low, hidden, gate_weight, up_weight, down_weight)
+    )(normed, meta, hidden, gate_weight, up_weight, down_weight)
 
 
 def on_device(
@@ -410,6 +553,17 @@
     top_count = expert_ids.shape[1]
     experts_all = lax.axis_size("sp") * lax.axis_size("tp")
     capacity = max(2, 2 * token_rows * top_count // experts_all)
+    if (
+        capacity % 16 == 0
+        and token_rows % HEAD == 0
+        and token_rows % capacity == 0
+        and experts_all % (token_rows // capacity) == 0
+    ):
+        meta = jnp.concatenate([expert_ids.astype(jnp.float32), route_weights], axis=1).T
+        meta = jnp.pad(meta, ((0, 8 - 2 * top_count), (0, 0)))
+        return run_experts(
+            normed, meta, hidden, gate_weight, up_weight, down_weight, capacity, top_count
+        )
     flat_ids = expert_ids.reshape(-1)
     order = jnp.arange(flat_ids.shape[0], dtype=jnp.int32)
     earlier = jnp.logical_and(
@@ -436,10 +590,6 @@
     )
     high = spread.astype(jnp.bfloat16)
     low = (spread - high.astype(jnp.float32)).astype(jnp.bfloat16)
-    if capacity % 16 == 0 and token_rows % capacity == 0 and experts_all % (token_rows // capacity) == 0:
-        return run_experts(
-            outgoing, high, low, hidden, gate_weight, up_weight, down_weight, capacity
-        )
     outgoing = outgoing.reshape(experts_all, capacity, normed.shape[1])
     arrived = lax.all_to_all(outgoing, ("sp", "tp"), split_axis=0, concat_axis=0, tiled=True)
     sources, slots, width = arrived.shape

time: 165 us -> 147 us (0.89)
  the two profiles are of different devices: /device:TPU:0 before, /device:TPU:5 now
where the time goes in v1:
time: 147 us; the launch traced here: 146 us
  Pallas kernels  140 us (95%)
  other arithmetic  3.6 us (2%)
  local copies, waits for them, and re-layouts  2.1 us (1%)
    pallas_call x1, Pallas kernels, run_experts(): pl.pallas_call(functools.partial(expert_kernel, n_sp, n_tp, capacity, top...  102 us
    pallas_call x1, Pallas kernels, attend(): pl.pallas_call(functools.partial(attention_kernel, n_sp, n_tp), out_shape...  38.7 us

profile of v1, /device:TPU:5, one launch (start us, length us, event | category | flops | bytes accessed | tf_op | source)
XLA Modules:
  0.0 146.4 jit_solution(10931786808868776892)
XLA Ops:
  0.0 0.0 copy-start.5
  0.0 0.2 fusion.7
  0.2 0.0 copy-start.11
  0.2 1.1 fusion.6
  1.4 0.1 copy.20
  1.5 0.1 copy.21
  1.6 0.0 copy-done.5
  1.6 0.2 copy.19
  1.8 0.1 multiply_reduce_fusion
  2.0 0.0 copy-done.11
  2.0 0.0 copy-start.8
  2.0 0.2 multiply_multiply_fusion
  2.2 0.2 subtract_convert_fusion
  2.4 0.0 copy-start.6
  2.4 0.0 copy-start.12
  2.5 0.2 copy-done.8
  2.8 0.0 copy-start.7
  2.8 0.0 copy-start.3
  2.8 0.0 copy-start.4
  2.8 0.1 pad_maximum_fusion.q_ref
  2.9 0.4 copy-done.6
  3.3 0.1 fusion
  3.5 0.0 copy-done.12
  3.5 0.1 fusion.2
  3.6 1.2 subtract_convert_fusion.1
  4.8 0.1 maximum_bitcast_fusion.1.k_ref
  4.9 0.0 copy-done.7
  5.0 0.1 copy.22
  5.1 0.0 copy-done.3
  5.1 0.0 copy-done.4
  5.1 0.0 copy-start.9
  5.1 0.0 copy-start.10
  5.1 0.0 copy-start
  5.1 0.0 copy-start.1
  5.1 0.0 copy-start.2
  5.2 38.7 %shard_map.136 = (bf16[128,2048]{1,0:T(8,128)(2,1)S(1)}, bf16[128,2048]{1,0:T(8,128)(2,1)S(1)}) custom-call(bf16[4,256,512]{2,1,0:T(8,128)(2,1)S(1)} %pad_maximum_fusion.q_ref, bf16[512,128]{1,0:T(8,128)(2,1)S(1)} %maximum_bitcast_fusion.1.k_ref, bf16[128,512]{1,0:T(8,128)(2,1)S(1)} %bitcast.17, f32[8,512]{1,0:T(8,128)S(1)} %broadcast_in_dim.13.doc_ref, ...), custom_call_target="tpu_custom_call" | custom-call | tf_op jit(solution)/shard_map/pallas_call | solution.py:213
  43.9 0.0 copy-done.9
  43.9 0.0 copy-done.10
  44.0 0.0 copy-done
  44.0 0.0 copy-done.1
  44.0 0.0 copy-done.2
  44.0 101.6 %shard_map.137 = bf16[128,2048]{1,0:T(8,128)(2,1)S(1)} custom-call(bf16[128,2048]{1,0:T(8,128)(2,1)S(1)} %get-tuple-element.7.nrm_ref, f32[8,128]{1,0:T(8,128)S(1)} %pad.4.meta_ref, bf16[128,2048]{1,0:T(8,128)(2,1)S(1)} %get-tuple-element.8.hid_ref, bf16[1,2048,512]{2,1,0:T(8,128)(2,1)S(1)} %copy-done, bf16[1,2048,512]{2,1,0:T(8,128)(2,1)S(1)} %copy-done.1, ...), custom_call_target="tpu_custom_call" | custom-call | tf_op jit(solution)/shard_map/pallas_call | solution.py:487
  145.6 0.8 copy.24
  (12 shorter events, 0.2 us)
Async XLA Ops:
  0.0 1.6 %copy-start.5 = (bf16[512,512]{1,0:T(8,128)(2,1)S(1)}, bf16[512,512]{1,0:T(8,128)(2,1)}, u32[]{:S(2)}) copy-start(bf16[512,512]{1,0:T(8,128)(2,1)} %param.15) | copy-start | bytes 1572868
  0.2 1.8 %copy-start.11 = (f32[128]{0:T(128)S(1)}, f32[128]{0:T(128)}, u32[]{:S(2)}) copy-start(f32[128]{0:T(128)} %param.18) | copy-start | bytes 1540
  2.0 0.7 copy-start.8
  2.4 0.9 copy-start.6
  2.4 1.1 copy-start.12
  2.8 2.2 %copy-start.7 = (bf16[512,128]{1,0:T(8,128)(2,1)S(1)}, bf16[512,128]{1,0:T(8,128)(2,1)}, u32[]{:S(2)}) copy-start(bf16[512,128]{1,0:T(8,128)(2,1)} %param.17) | copy-start | bytes 393220
  2.8 2.3 %copy-start.3 = (bf16[128,2048]{1,0:T(8,128)(2,1)S(1)}, bf16[128,2048]{1,0:T(8,128)(2,1)}, u32[]{:S(2)}) copy-start(bf16[128,2048]{1,0:T(8,128)(2,1)} %res_ref.1) | copy-start | bytes 1572868
  2.8 2.3 %copy-start.4 = (f32[2048]{0:T(1024)S(1)}, f32[2048]{0:T(1024)}, u32[]{:S(2)}) copy-start(f32[2048]{0:T(1024)} %param.22) | copy-start | bytes 24580
  5.1 38.8 %copy-start.9 = (s32[128,2]{0,1:T(2,128)S(1)}, s32[128,2]{0,1:T(2,128)}, u32[]{:S(2)}) copy-start(s32[128,2]{0,1:T(2,128)} %param.23) | copy-start | bytes 3076
  5.1 38.8 %copy-start.10 = (f32[128,2]{0,1:T(2,128)S(1)}, f32[128,2]{0,1:T(2,128)}, u32[]{:S(2)}) copy-start(f32[128,2]{0,1:T(2,128)} %param.24) | copy-start | bytes 3076
  5.1 38.8 %copy-start = (bf16[1,2048,512]{2,1,0:T(8,128)(2,1)S(1)}, bf16[1,2048,512]{2,1,0:T(8,128)(2,1)}, u32[]{:S(2)}) copy-start(bf16[1,2048,512]{2,1,0:T(8,128)(2,1)} %gate_hbm.1) | copy-start | bytes 6291460
  5.1 38.8 %copy-start.1 = (bf16[1,2048,512]{2,1,0:T(8,128)(2,1)S(1)}, bf16[1,2048,512]{2,1,0:T(8,128)(2,1)}, u32[]{:S(2)}) copy-start(bf16[1,2048,512]{2,1,0:T(8,128)(2,1)} %up_hbm.1) | copy-start | bytes 6291460
  5.1 38.8 %copy-start.2 = (bf16[1,512,2048]{2,1,0:T(8,128)(2,1)S(1)}, bf16[1,512,2048]{2,1,0:T(8,128)(2,1)}, u32[]{:S(2)}) copy-start(bf16[1,512,2048]{2,1,0:T(8,128)(2,1)} %down_hbm.1) | copy-start | bytes 6291460

commit v2 on v0

--- a/solution.py
+++ b/solution.py
@@ -19,7 +19,765 @@
 MESH = pl.DeviceIdType.MESH
 DOC_KEY = 128.0
 DOC_QUERY = 64.0
+PIECES = 2
+OFFSETS = (1, -2, 2, -1, 3, -3)
 EXP2_SCALE = math.log2(math.e) / math.sqrt(HEAD)
+
+
+def layer_kernel(
+    n_sp, n_tp, capacity, top_count,
+    q_ref, k_ref, v_ref, doc_ref, qg_ref, kg_ref, ids_ref, rw_ref, res_ref, gain_ref,
+    wo_hbm, gate_hbm, up_hbm, down_hbm,
+    new_ref,
+    wo_v, gate_v, up_v, down_v, cos_s, sin_s, meta_s, q_aug, k_own, k_in, v_in, doc_in,
+    k_aug, vt_s, m_s, l_s, acc_s, att_s, all_s, hid_s, nrm_s,
+    metas, blocks, picked, arrived, answer, homing, returned, spread, total_s,
+    back, joined, midway, summed,
+    k_send, k_recv, v_send, v_recv, c_send, c_recv, t_send, t_recv,
+    m_send, m_recv, z_send, z_recv, d_send, d_recv, h_send, h_recv, r_send, r_recv,
+    b_send, b_recv, j_send, y_recv, s_recv, w_sem,
+):
+    devices = n_sp * n_tp
+    rows = res_ref.shape[0]
+    members = rows // capacity
+    groups = devices // members
+    piece = rows // PIECES
+    sp = lax.axis_index("sp")
+    tp = lax.axis_index("tp")
+    me = sp * n_tp + tp
+    plane = lax.div(me, members)
+    pos = lax.rem(me, members)
+
+    loads = [
+        pltpu.make_async_copy(source.at[0], into, w_sem.at[i])
+        for i, (source, into) in enumerate(
+            ((gate_hbm, gate_v), (up_hbm, up_v), (down_hbm, down_v))
+        )
+    ]
+
+    def place(device):
+        return (lax.div(device, n_tp), lax.rem(device, n_tp))
+
+    def region(index):
+        return pl.ds(pl.multiple_of(index * capacity, capacity), capacity)
+
+    def level(block):
+        return jnp.logical_and(block >= 0, block < groups)
+
+    length = k_ref.shape[0]
+    heads = q_ref.shape[1] // HEAD
+    width = att_s.shape[1]
+    slots = len(OFFSETS)
+    half = HEAD // 2
+    side = 1 - 2 * lax.rem(sp, 2)
+    across, ahead, behind = sp + side, sp + 2 * side, sp - 2 * side
+
+    def inside(index):
+        return jnp.logical_and(index >= 0, index < n_sp)
+
+    has_ahead, has_behind = inside(ahead), inside(behind)
+    has_spare = inside(sp + 4 * side)
+
+    def offset(j):
+        return sum(jnp.where(j == i, o, 0) for i, o in enumerate(OFFSETS))
+
+    def exists(j):
+        return inside(sp + side * offset(j))
+
+    def reader(j):
+        odd = OFFSETS[j] % 2 == 1
+        return sp + side * OFFSETS[j] if odd else sp - side * OFFSETS[j]
+
+    wo_copy = pltpu.make_async_copy(wo_hbm, wo_v, w_sem.at[3])
+    wo_copy.start()
+    for load in loads:
+        load.start()
+
+    barrier = pltpu.get_barrier_semaphore()
+
+    def greet(i, carry):
+        there = lax.rem(me + i, devices)
+        pl.semaphore_signal(barrier, inc=1, device_id=place(there), device_id_type=MESH)
+        return carry
+
+    lax.fori_loop(1, devices, greet, 0)
+
+    def column(row):
+        return jnp.broadcast_to(row, (HEAD, HEAD)).T[:, :1]
+
+    freq_count = HEAD // 4
+    exponent = lax.broadcasted_iota(jnp.int32, (freq_count, 1), 0).astype(jnp.float32) / freq_count
+    inverse = jnp.exp2(exponent * -math.log2(rope_base))
+    position = sp * length + lax.broadcasted_iota(jnp.int32, (1, length), 1)
+    grid_row = lax.div(position, GRID_W).astype(jnp.float32)
+    grid_col = lax.rem(position, GRID_W).astype(jnp.float32)
+    angles = jnp.concatenate([inverse * grid_row, inverse * grid_col], axis=0)
+    cos_s[...] = jnp.cos(angles)
+    sin_s[...] = jnp.sin(angles)
+
+    def turned(projected, gains):
+        wide = projected.astype(jnp.float32).T
+        scaled = (
+            wide * lax.rsqrt(jnp.mean(wide * wide, axis=0, keepdims=True) + norm_eps) * gains
+        )
+        upper, lower = scaled[:half], scaled[half:]
+        cosine, sine = cos_s[...], sin_s[...]
+        return jnp.concatenate(
+            [upper * cosine - lower * sine, upper * sine + lower * cosine], axis=0
+        )
+
+    k_own[...] = turned(k_ref[...], column(kg_ref[...])).T.astype(jnp.bfloat16)
+    for k in range(top_count):
+        for r, table in ((k, ids_ref), (top_count + k, rw_ref)):
+            meta_s[r : r + 1, :] = table[k : k + 1, :].astype(jnp.float32)
+    pl.semaphore_wait(barrier, devices - 1)
+
+    def shift(source, into, sends, receives, i, there):
+        return pltpu.make_async_remote_copy(
+            src_ref=source,
+            dst_ref=into.at[i],
+            send_sem=sends.at[i],
+            recv_sem=receives.at[i],
+            device_id=(there, tp),
+            device_id_type=MESH,
+        )
+
+    key_plan = (
+        (k_own, across, True),
+        (k_own, ahead, has_ahead),
+        (k_own, behind, has_behind),
+        (k_in.at[0], ahead, has_ahead),
+        (k_in.at[0], behind, has_behind),
+        (k_in.at[3], ahead, jnp.logical_and(has_ahead, has_behind)),
+    )
+    value_plan = (
+        (v_ref, across, True),
+        (v_ref, ahead, has_ahead),
+        (v_ref, behind, has_behind),
+        (v_in.at[2], across, has_ahead),
+        (v_in.at[1], across, has_behind),
+        (v_in.at[6], across, has_spare),
+        (v_in.at[2], behind, jnp.logical_and(has_ahead, has_behind)),
+    )
+
+    def key_shift(i):
+        return shift(key_plan[i][0], k_in, k_send, k_recv, i, key_plan[i][1])
+
+    def value_shift(i):
+        return shift(value_plan[i][0], v_in, v_send, v_recv, i, value_plan[i][1])
+
+    def on(allowed, act):
+        if allowed is True:
+            act()
+        elif allowed is not False:
+            pl.when(allowed)(act)
+
+    def start_keys(*which):
+        for i in which:
+            on(key_plan[i][2], lambda: key_shift(i).start())
+
+    def start_values(*which):
+        for i in which:
+            on(value_plan[i][2], lambda: value_shift(i).start())
+
+    def key_wait(j):
+        shift(k_own, k_in, k_send, k_recv, j, sp).wait_recv()
+
+    def value_wait(j):
+        shift(v_ref, v_in, v_send, v_recv, j, sp).wait_recv()
+
+    def doc_shift(j):
+        return shift(doc_ref, doc_in, c_send, c_recv, j, reader(j))
+
+    for j in range(slots):
+        pl.when(inside(reader(j)))(lambda: doc_shift(j).start())
+    start_keys(0, 1, 2)
+    start_values(0, 1, 2)
+
+    query_gains = column(qg_ref[...])
+    for h in range(heads):
+        q_aug[h, :HEAD, :] = turned(
+            q_ref[:, h * HEAD : (h + 1) * HEAD], query_gains
+        ).astype(jnp.bfloat16)
+        labels = lax.broadcasted_iota(jnp.int32, (HEAD, length), 0)
+        q_aug[h, HEAD:, :] = jnp.where(doc_ref[...] == labels, DOC_QUERY, 0.0).astype(
+            jnp.bfloat16
+        )
+
+    def take(keys, values, docs, first):
+        doc_col = jnp.broadcast_to(docs[...].astype(jnp.float32), (HEAD, length)).T
+        lanes = lax.broadcasted_iota(jnp.int32, (length, HEAD), 1).astype(jnp.float32)
+        k_aug[:, :HEAD] = keys[...]
+        k_aug[:, HEAD:] = jnp.where(doc_col == lanes, DOC_KEY, 0.0).astype(jnp.bfloat16)
+        vt_s[...] = values[...].T
+        for h in range(heads):
+            s = jnp.dot(k_aug[...], q_aug[h], preferred_element_type=jnp.float32)
+            top = jnp.max(s, axis=0, keepdims=True)
+            if not first:
+                top = jnp.maximum(m_s[h], top)
+            e = jnp.exp2((s - top) * EXP2_SCALE)
+            den = jnp.sum(e, axis=0, keepdims=True)
+            part = jnp.dot(
+                vt_s[...], e.astype(jnp.bfloat16), preferred_element_type=jnp.float32
+            )
+            if first:
+                l_s[h] = den
+                acc_s[h] = part
+            else:
+                old = jnp.exp2((m_s[h] - top) * EXP2_SCALE)
+                l_s[h] = l_s[h] * old + den
+                acc_s[h] = acc_s[h] * old + part
+            m_s[h] = top
+
+    take(k_own, v_ref, doc_ref, True)
+
+    key_wait(0)
+    start_keys(3, 4)
+
+    @pl.when(has_ahead)
+    def _():
+        value_wait(2)
+        start_values(3, 6)
+
+    @pl.when(has_behind)
+    def _():
+        value_wait(1)
+        start_values(4)
+
+    def step(j, carry):
+        @pl.when(exists(j))
+        def _():
+            @pl.when(jnp.logical_and(j != 0, j != 3))
+            def _():
+                key_wait(j)
+
+            @pl.when(jnp.logical_and(j != 1, j != 2))
+            def _():
+                value_wait(j)
+
+            shift(doc_ref, doc_in, c_send, c_recv, j, sp).wait_recv()
+            take(k_in.at[j], v_in.at[j], doc_in.at[j], False)
+
+        @pl.when(jnp.logical_and(j == 1, has_behind))
+        def _():
+            key_wait(3)
+            start_keys(5)
+
+        @pl.when(jnp.logical_and(j == 2, has_spare))
+        def _():
+            value_wait(6)
+            start_values(5)
+
+        return carry
+
+    lax.fori_loop(0, slots, step, 0)
+
+    for h in range(heads):
+        out = acc_s[h] / l_s[h]
+        att_s[:, h * HEAD : (h + 1) * HEAD] = out.T.astype(jnp.bfloat16)
+
+    def exchange(k):
+        there = lax.rem(tp + k, n_tp)
+        return pltpu.make_async_remote_copy(
+            src_ref=att_s.at[pl.ds(pl.multiple_of(there * rows, rows), rows), :],
+            dst_ref=all_s.at[tp],
+            send_sem=t_send.at[k],
+            recv_sem=t_recv.at[k],
+            device_id=(sp, there),
+            device_id_type=MESH,
+        )
+
+    for k in range(n_tp - 1, 0, -1):
+        exchange(k).start()
+    wo_copy.wait()
+
+    def weight_rows(i):
+        return wo_v[pl.ds(pl.multiple_of(i * width, width), width), :]
+
+    projected = jnp.dot(
+        att_s[pl.ds(pl.multiple_of(tp * rows, rows), rows), :],
+        weight_rows(tp),
+        preferred_element_type=jnp.float32,
+    )
+    for k in range(1, n_tp):
+        exchange(k).wait_recv()
+        source = lax.rem(tp - k + n_tp, n_tp)
+        projected += jnp.dot(
+            all_s[source], weight_rows(source), preferred_element_type=jnp.float32
+        )
+    hidden = (res_ref[...].astype(jnp.float32) + projected).astype(jnp.bfloat16)
+    hid_s[...] = hidden
+    wide = hidden.astype(jnp.float32)
+    mean = jnp.mean(wide * wide, axis=-1, keepdims=True)
+    nrm_s[...] = (wide * lax.rsqrt(mean + norm_eps) * gain_ref[...]).astype(jnp.bfloat16)
+
+    def tell(i, block):
+        return pltpu.make_async_remote_copy(
+            src_ref=meta_s,
+            dst_ref=metas.at[block],
+            send_sem=m_send.at[i],
+            recv_sem=m_recv.at[block],
+            device_id=place(lax.rem(plane + i, groups) * members + pos),
+            device_id_type=MESH,
+        )
+
+    def pass_on(source, block, way, c):
+        part = pl.ds(c * piece, piece)
+        return pltpu.make_async_remote_copy(
+            src_ref=source.at[part],
+            dst_ref=blocks.at[block, part],
+            send_sem=z_send.at[way, block, c],
+            recv_sem=z_recv.at[block, c],
+            device_id=place(me + (2 * way - 1) * members),
+            device_id_type=MESH,
+        )
+
+    def dispatch(block, peer, landing):
+        return pltpu.make_async_remote_copy(
+            src_ref=picked.at[block, region(peer)],
+            dst_ref=arrived.at[block, region(landing)],
+            send_sem=d_send.at[block, peer],
+            recv_sem=d_recv.at[block, landing],
+            device_id=place(plane * members + peer),
+            device_id_type=MESH,
+        )
+
+    def give_home(block, origin, c):
+        part = pl.ds(c * piece, piece)
+        return pltpu.make_async_remote_copy(
+            src_ref=answer.at[block, part],
+            dst_ref=homing.at[origin, part],
+            send_sem=h_send.at[block, c],
+            recv_sem=h_recv.at[origin, c],
+            device_id=place(block * members + pos),
+            device_id_type=MESH,
+        )
+
+    def give_back(source, origin, member, landing):
+        return pltpu.make_async_remote_copy(
+            src_ref=source.at[region(member)],
+            dst_ref=returned.at[region(origin * members + landing)],
+            send_sem=r_send.at[origin, member],
+            recv_sem=r_recv.at[origin, landing],
+            device_id=place(plane * members + member),
+            device_id_type=MESH,
+        )
+
+    def give_across(block, member, landing):
+        return pltpu.make_async_remote_copy(
+            src_ref=answer.at[block, region(member)],
+            dst_ref=back.at[block, region(landing)],
+            send_sem=b_send.at[block, member],
+            recv_sem=b_recv.at[block, landing],
+            device_id=place(plane * members + member),
+            device_id_type=MESH,
+        )
+
+    def give_next(block, way, c):
+        part = pl.ds(c * piece, piece)
+        return pltpu.make_async_remote_copy(
+            src_ref=joined.at[block, part],
+            dst_ref=midway.at[way, part],
+            send_sem=j_send.at[block, c],
+            recv_sem=y_recv.at[way, c],
+            device_id=place(me + (1 - 2 * way) * members),
+            device_id_type=MESH,
+        )
+
+    def give_sum(block, way, c):
+        part = pl.ds(c * piece, piece)
+        return pltpu.make_async_remote_copy(
+            src_ref=joined.at[block, part],
+            dst_ref=summed.at[way, part],
+            send_sem=j_send.at[block, c],
+            recv_sem=s_recv.at[way, c],
+            device_id=place(block * members + pos),
+            device_id_type=MESH,
+        )
+
+    def others(act, first=1):
+        def one(i, carry):
+            act(lax.rem(pos + i, members))
+            return carry
+
+        lax.fori_loop(first, members, one, 0)
+
+    for i in range(1, groups):
+        tell(i, plane).start()
+    for way in range(2):
+
+        @pl.when(level(plane + 2 * way - 1))
+        def _():
+            for c in range(PIECES):
+                pass_on(nrm_s, plane, way, c).start()
+
+    def slot_rows(meta):
+        experts = lax.broadcasted_iota(jnp.int32, (devices, rows), 0).astype(jnp.float32)
+        hits = [experts == meta[k : k + 1, :] for k in range(top_count)]
+        named = sum(hit.astype(jnp.float32) for hit in hits)
+        ahead = (
+            lax.broadcasted_iota(jnp.int32, (rows, rows), 0)
+            < lax.broadcasted_iota(jnp.int32, (rows, rows), 1)
+        )
+        before = jnp.dot(
+            named.astype(jnp.bfloat16),
+            ahead.astype(jnp.float32).astype(jnp.bfloat16),
+            preferred_element_type=jnp.float32,
+        )
+        return [
+            meta[k : k + 1, :] * capacity
+            + jnp.sum(jnp.where(hits[k], before, 0.0), axis=0, keepdims=True)
+            for k in range(top_count)
+        ]
+
+    def slot_numbers(group):
+        return (
+            lax.broadcasted_iota(jnp.int32, (rows, rows), 0) + group * rows
+        ).astype(jnp.float32)
+
+    def gather(source, meta, block):
+        numbers = slot_numbers(plane)
+        choice = sum((numbers == row).astype(jnp.float32) for row in slot_rows(meta))
+        picked[block] = jnp.dot(
+            choice.astype(jnp.bfloat16), source[...], preferred_element_type=jnp.float32
+        ).astype(jnp.bfloat16)
+        others(lambda peer: dispatch(block, peer, pos).start())
+        arrived[block, region(pos), :] = picked[block, region(pos), :]
+
+    def expert(block):
+        others(lambda peer: dispatch(block, peer, peer).wait_recv())
+        x = arrived[block]
+        gate_part = jnp.dot(x, gate_v[...], preferred_element_type=jnp.float32)
+        up_part = jnp.dot(x, up_v[...], preferred_element_type=jnp.float32)
+        activity = (jax.nn.silu(gate_part) * up_part).astype(jnp.bfloat16)
+        answer[block] = jnp.dot(
+            activity, down_v[...], preferred_element_type=jnp.float32
+        ).astype(jnp.bfloat16)
+
+    def both_ways(distance, act):
+        def one(way, carry):
+            block = plane - (2 * way - 1) * distance
+
+            @pl.when(level(block))
+            def _():
+                act(block, way)
+
+            return carry
+
+        lax.fori_loop(0, 2, one, 0)
+
+    gather(nrm_s, meta_s[...], plane)
+    own_slots = slot_rows(meta_s[...])
+    for g in range(groups):
+        numbers = slot_numbers(g)
+        weights = sum(
+            jnp.where(numbers == own_slots[k], meta_s[top_count + k : top_count + k + 1, :], 0.0)
+            for k in range(top_count)
+        ).T
+        high = weights.astype(jnp.bfloat16)
+        spread[g, 0] = high
+        spread[g, 1] = (weights - high.astype(jnp.float32)).astype(jnp.bfloat16)
+    for load in loads:
+        load.wait()
+
+    def receive(block, way, c):
+        pass_on(nrm_s, block, way, c).wait_recv()
+
+        @pl.when(level(plane + 2 * way - 1))
+        def _():
+            pass_on(blocks.at[block], block, way, c).start()
+
+    def collect(block, way):
+        tell(1, block).wait_recv()
+        gather(blocks.at[block], metas[block], block)
+
+    def beyond(way):
+        return level(plane - (1 - 2 * way))
+
+    def past(block, way):
+        return level(block + (1 - 2 * way))
+
+    def relayed(distance, far):
+        return far if distance == 2 else distance == 3
+
+    def serve(block, way, distance):
+        expert(block)
+        joint = relayed(distance, beyond(way))
+
+        def raw():
+            for c in range(PIECES):
+                give_home(block, plane, c).start()
+
+        def through():
+            others(lambda member: give_across(block, member, pos).start())
+            back[block, region(pos), :] = answer[block, region(pos), :]
+
+        if joint is True:
+            through()
+        elif joint is False:
+            raw()
+        else:
+            pl.when(joint)(through)
+            pl.when(jnp.logical_not(joint))(raw)
+
+    def join(block):
+        others(lambda member: give_across(block, member, member).wait_recv())
+        meta = metas[block]
+        numbers = slot_numbers(plane)
+        lines = slot_rows(meta)
+        weights = sum(
+            jnp.where(numbers == lines[k], meta[top_count + k : top_count + k + 1, :], 0.0)
+            for k in range(top_count)
+        ).T
+        high = weights.astype(jnp.bfloat16)
+        low = (weights - high.astype(jnp.float32)).astype(jnp.bfloat16)
+        joined[block] = (
+            jnp.dot(high, back[block], preferred_element_type=jnp.float32)
+            + jnp.dot(low, back[block], preferred_element_type=jnp.float32)
+        ).astype(jnp.bfloat16)
+
+    def begin_chain(block, way):
+        join(block)
+        for c in range(PIECES):
+            give_next(block, way, c).start()
+
+    def extend_chain(block, way):
+        @pl.when(beyond(way))
+        def _():
+            join(block)
+            for c in range(PIECES):
+                part = pl.ds(c * piece, piece)
+                give_next(block, way, c).wait_recv()
+                joined[block, part, :] = (
+                    joined[block, part, :].astype(jnp.float32)
+                    + midway[way, part, :].astype(jnp.float32)
+                ).astype(jnp.bfloat16)
+                give_sum(block, way, c).start()
+
+    def serve_at(distance):
+        both_ways(distance, functools.partial(serve, distance=distance))
+
+    def share(origin, way, distance):
+        def pieces():
+            for c in range(PIECES):
+                give_home(origin, origin, c).wait_recv()
+                for i in range(c * members // PIECES, (c + 1) * members // PIECES):
+
+                    @pl.when(pos != i)
+                    def _():
+                        give_back(homing.at[origin], origin, i, pos).start()
+
+            returned[region(origin * members + pos), :] = homing[origin, region(pos), :]
+
+        on(raw_from(origin, way, distance), pieces)
+
+    def raw_from(origin, way, distance):
+        joint = relayed(distance, level(origin - (2 * way - 1)))
+        return not joint if isinstance(joint, bool) else jnp.logical_not(joint)
+
+    def share_at(distance):
+        if distance != 3:
+            both_ways(distance, functools.partial(share, distance=distance))
+
+    for distance in range(1, groups):
+        for c in range(PIECES):
+            if c == PIECES - 1:
+                if distance == 1:
+                    expert(plane)
+                    others(lambda member: give_back(answer.at[plane], plane, member, pos).start())
+                    returned[region(me), :] = answer[plane, region(pos), :]
+                else:
+                    serve_at(distance - 1)
+            both_ways(distance, functools.partial(receive, c=c))
+        both_ways(distance, collect)
+        if distance > 2:
+            share_at(distance - 2)
+    serve_at(groups - 1)
+    if groups > 3:
+        both_ways(3, begin_chain)
+    share_at(max(1, groups - 2))
+    both_ways(2, extend_chain)
+    share_at(groups - 1)
+
+    total = hid_s[...].astype(jnp.float32)
+
+    def combine(group):
+        back = returned[pl.ds(pl.multiple_of(group * rows, rows), rows), :]
+        part = jnp.dot(spread[group, 0], back, preferred_element_type=jnp.float32)
+        return part + jnp.dot(spread[group, 1], back, preferred_element_type=jnp.float32)
+
+    def gathered(origin):
+        others(lambda member: give_back(homing.at[origin], origin, member, member).wait_recv())
+        return combine(origin)
+
+    total_s[...] = total + gathered(plane)
+
+    def add(origin, way, distance):
+        def slots_back():
+            total_s[...] += gathered(origin)
+
+        def sum_back():
+            for c in range(PIECES):
+                give_sum(origin, 1 - way, c).wait_recv()
+            total_s[...] += summed[1 - way].astype(jnp.float32)
+
+        raw = raw_from(origin, way, distance)
+        on(raw, slots_back)
+        if distance == 2:
+            pl.when(jnp.logical_not(raw))(sum_back)
+
+    for distance in range(1, groups):
+        if distance != 3:
+            both_ways(distance, functools.partial(add, distance=distance))
+    new_ref[...] = total_s[...].astype(jnp.bfloat16)
+
+    for i in range(1, groups):
+        tell(i, plane).wait_send()
+    for way in range(2):
+
+        @pl.when(level(plane + 2 * way - 1))
+        def _():
+            for c in range(PIECES):
+                pass_on(nrm_s, plane, way, c).wait_send()
+
+    def sent(block, way, distance):
+        @pl.when(level(plane + 2 * way - 1))
+        def _():
+            for c in range(PIECES):
+                pass_on(nrm_s, block, way, c).wait_send()
+
+        others(lambda peer: dispatch(block, peer, pos).wait_send())
+
+        def shared():
+            others(lambda member: give_back(homing.at[block], block, member, pos).wait_send())
+
+        def raw():
+            for c in range(PIECES):
+                give_home(block, plane, c).wait_send()
+
+        def through():
+            others(lambda member: give_across(block, member, pos).wait_send())
+            for c in range(PIECES):
+                give_next(block, way, c).wait_send()
+
+        if distance != 3:
+            on(raw_from(block, way, distance), shared)
+        joint = relayed(distance, beyond(way))
+        if joint is True:
+            through()
+        elif joint is False:
+            raw()
+        else:
+            pl.when(joint)(through)
+            pl.when(jnp.logical_not(joint))(raw)
+
+    others(lambda peer: dispatch(plane, peer, pos).wait_send())
+    others(lambda member: give_back(answer.at[plane], plane, member, pos).wait_send())
+    for distance in range(1, groups):
+        both_ways(distance, functools.partial(sent, distance=distance))
+
+
+    for i in range(slots):
+        on(key_plan[i][2], lambda: key_shift(i).wait_send())
+        pl.when(inside(reader(i)))(lambda: doc_shift(i).wait_send())
+    for i in range(slots + 1):
+        on(value_plan[i][2], lambda: value_shift(i).wait_send())
+    for k in range(1, n_tp):
+        exchange(k).wait_send()
+
+
+def run_layer(
+    query_proj, key_proj, value_proj, docs, query_gain, key_gain, expert_ids, route_weights,
+    residual, norm_gain, output_weight, gate_weight, up_weight, down_weight, capacity,
+):
+    n_sp, n_tp = lax.axis_size("sp"), lax.axis_size("tp")
+    length = key_proj.shape[0]
+    heads = query_proj.shape[1] // HEAD
+    rows, model = residual.shape
+    top_count = expert_ids.shape[0]
+    members = rows // capacity
+    groups = n_sp * n_tp // members
+    slots = len(OFFSETS)
+    block = (length, HEAD)
+    narrow = jnp.bfloat16
+    vmem = pl.BlockSpec(memory_space=pltpu.VMEM)
+    anywhere = pl.BlockSpec(memory_space=pl.ANY)
+    buffer = pltpu.VMEM((groups, rows, model), narrow)
+    dma = pltpu.SemaphoreType.DMA
+    return pl.pallas_call(
+        functools.partial(layer_kernel, n_sp, n_tp, capacity, top_count),
+        out_shape=jax.ShapeDtypeStruct(residual.shape, narrow),
+        in_specs=[vmem] * 10 + [anywhere] * 4,
+        out_specs=vmem,
+        scratch_shapes=[
+            pltpu.VMEM(output_weight.shape, narrow),
+            pltpu.VMEM(gate_weight.shape[1:], narrow),
+            pltpu.VMEM(up_weight.shape[1:], narrow),
+            pltpu.VMEM(down_weight.shape[1:], narrow),
+            pltpu.VMEM((HEAD // 2, length), jnp.float32),
+            pltpu.VMEM((HEAD // 2, length), jnp.float32),
+            pltpu.VMEM((8, rows), jnp.float32),
+            pltpu.VMEM((heads, 2 * HEAD, length), narrow),
+            pltpu.VMEM(block, narrow),
+            pltpu.VMEM((slots,) + block, narrow),
+            pltpu.VMEM((slots + 1,) + block, narrow),
+            pltpu.VMEM((slots,) + docs.shape, jnp.int32),
+            pltpu.VMEM((length, 2 * HEAD), narrow),
+            pltpu.VMEM((HEAD, length), narrow),
+            pltpu.VMEM((heads, 1, length), jnp.float32),
+            pltpu.VMEM((heads, 1, length), jnp.float32),
+            pltpu.VMEM((heads, HEAD, length), jnp.float32),
+            pltpu.VMEM((length, heads * HEAD), narrow),
+            pltpu.VMEM((n_tp, rows, heads * HEAD), narrow),
+            pltpu.VMEM((rows, model), narrow),
+            pltpu.VMEM((rows, model), narrow),
+            pltpu.VMEM((groups, 8, rows), jnp.float32),
+            buffer,
+            buffer,
+            buffer,
+            buffer,
+            buffer,
+            pltpu.VMEM((groups * rows, model), narrow),
+            pltpu.VMEM((groups, 2, rows, rows), narrow),
+            pltpu.VMEM((rows, model), jnp.float32),
+            buffer,
+            buffer,
+            pltpu.VMEM((2, rows, model), narrow),
+            pltpu.VMEM((2, rows, model), narrow),
+            dma((slots,)),
+            dma((slots,)),
+            dma((slots + 1,)),
+            dma((slots + 1,)),
+            dma((slots,)),
+            dma((slots,)),
+            dma((n_tp,)),
+            dma((n_tp,)),
+            dma((groups,)),
+            dma((groups,)),
+            dma((2, groups, PIECES)),
+            dma((groups, PIECES)),
+            dma((groups, members)),
+            dma((groups, members)),
+            dma((groups, PIECES)),
+            dma((groups, PIECES)),
+            dma((groups, members)),
+            dma((groups, members)),
+            dma((groups, members)),
+            dma((groups, members)),
+            dma((groups, PIECES)),
+            dma((2, PIECES)),
+            dma((2, PIECES)),
+            dma((4,)),
+        ],
+        compiler_params=pltpu.CompilerParams(
+            collective_id=1, has_side_effects=True, vmem_limit_bytes=60 * 1024 * 1024
+        ),
+    )(
+        query_proj, key_proj, value_proj, docs,
+        query_gain.reshape(1, -1), key_gain.reshape(1, -1), expert_ids, route_weights,
+        residual, norm_gain.reshape(1, -1),
+        output_weight, gate_weight, up_weight, down_weight,
+    )
 
 
 def rotary_tables(first_row, length):
@@ -237,143 +995,7 @@
     )(q_aug, key_norm, value_t, doc_rows, residual, norm_gain.reshape(1, -1), output_weight)
 
 
-def expert_kernel(
-    n_tp, capacity, out_ref, high_ref, low_ref, hid_ref, gate_hbm, up_hbm, down_hbm,
-    new_ref,
-    gate_v, up_v, down_v, arrived, answer, returned,
-    d_send, d_recv, r_send, r_recv, w_sem,
-):
-    me = lax.axis_index("sp") * n_tp + lax.axis_index("tp")
-    devices = out_ref.shape[0] // capacity
-    rows = hid_ref.shape[0]
-    members = rows // capacity
-    groups = devices // members
-    my_group = lax.div(me, members)
-    my_place = lax.rem(me, members)
-
-    loads = [
-        pltpu.make_async_copy(source.at[0], into, w_sem.at[i])
-        for i, (source, into) in enumerate(
-            ((gate_hbm, gate_v), (up_hbm, up_v), (down_hbm, down_v))
-        )
-    ]
-    for load in loads:
-        load.start()
-
-    def place(device):
-        return (lax.div(device, n_tp), lax.rem(device, n_tp))
-
-    def slots(device):
-        return pl.ds(pl.multiple_of(device * capacity, capacity), capacity)
-
-    barrier = pltpu.get_barrier_semaphore()
-
-    def greet(i, carry):
-        there = lax.rem(me + i, devices)
-        pl.semaphore_signal(barrier, inc=1, device_id=place(there), device_id_type=MESH)
-        return carry
-
-    lax.fori_loop(1, devices, greet, 0)
-    pl.semaphore_wait(barrier, devices - 1)
-
-    def dispatch(device, landing):
-        return pltpu.make_async_remote_copy(
-            src_ref=out_ref.at[slots(device)],
-            dst_ref=arrived.at[slots(landing)],
-            send_sem=d_send.at[device],
-            recv_sem=d_recv.at[landing],
-            device_id=place(device),
-            device_id_type=MESH,
-        )
-
-    def give_back(device, landing):
-        return pltpu.make_async_remote_copy(
-            src_ref=answer.at[slots(device)],
-            dst_ref=returned.at[slots(landing)],
-            send_sem=r_send.at[device],
-            recv_sem=r_recv.at[landing],
-            device_id=place(device),
-            device_id_type=MESH,
-        )
-
-    def each(group, skip_self, act):
-        def one(i, carry):
-            act(group * members + lax.rem(my_place + i, members))
-            return carry
-
-        lax.fori_loop(1 if skip_self else 0, members, one, 0)
-
-    def group_at(step):
-        return lax.rem(my_group + step + groups, groups)
-
-    def group_rows(group):
-        return pl.ds(pl.multiple_of(group * rows, rows), rows)
-
-    for c in range(groups):
-        each(group_at(c), c == 0, lambda device: dispatch(device, me).start())
-    arrived[slots(me), :] = out_ref[slots(me), :]
-    for load in loads:
-        load.wait()
-
-    for c in range(groups):
-        group = group_at(-c)
-        each(group, c == 0, lambda device: dispatch(device, device).wait_recv())
-        x = arrived[group_rows(group), :]
-        gate_part = jnp.dot(x, gate_v[...], preferred_element_type=jnp.float32)
-        up_part = jnp.dot(x, up_v[...], preferred_element_type=jnp.float32)
-        activity = (jax.nn.silu(gate_part) * up_part).astype(jnp.bfloat16)
-        answer[group_rows(group), :] = jnp.dot(
-            activity, down_v[...], preferred_element_type=jnp.float32
-        ).astype(jnp.bfloat16)
-        each(group, c == 0, lambda device: give_back(device, me).start())
-    returned[slots(me), :] = answer[slots(me), :]
-
-    total = hid_ref[...].astype(jnp.float32)
-    for c in range(groups):
-        group = group_at(c)
-        each(group, c == 0, lambda device: give_back(device, device).wait_recv())
-        back = returned[group_rows(group), :]
-        lanes = group_rows(group)
-        total += jnp.dot(high_ref[:, lanes], back, preferred_element_type=jnp.float32)
-        total += jnp.dot(low_ref[:, lanes], back, preferred_element_type=jnp.float32)
-    new_ref[...] = total.astype(jnp.bfloat16)
-
-    for c in range(groups):
-        each(group_at(c), c == 0, lambda device: dispatch(device, me).wait_send())
-        each(group_at(c), c == 0, lambda device: give_back(device, me).wait_send())
-
-
-def run_experts(outgoing, high, low, hidden, gate_weight, up_weight, down_weight, capacity):
-    n_tp = lax.axis_size("tp")
-    devices = outgoing.shape[0] // capacity
-    vmem = pl.BlockSpec(memory_space=pltpu.VMEM)
-    anywhere = pl.BlockSpec(memory_space=pl.ANY)
-    buffer = pltpu.VMEM(outgoing.shape, jnp.bfloat16)
-    return pl.pallas_call(
-        functools.partial(expert_kernel, n_tp, capacity),
-        out_shape=jax.ShapeDtypeStruct(hidden.shape, jnp.bfloat16),
-        in_specs=[vmem] * 4 + [anywhere] * 3,
-        out_specs=vmem,
-        scratch_shapes=[
-            pltpu.VMEM(gate_weight.shape[1:], jnp.bfloat16),
-            pltpu.VMEM(up_weight.shape[1:], jnp.bfloat16),
-            pltpu.VMEM(down_weight.shape[1:], jnp.bfloat16),
-            buffer,
-            buffer,
-            buffer,
-            pltpu.SemaphoreType.DMA((devices,)),
-            pltpu.SemaphoreType.DMA((devices,)),
-            pltpu.SemaphoreType.DMA((devices,)),
-            pltpu.SemaphoreType.DMA((devices,)),
-            pltpu.SemaphoreType.DMA((3,)),
-        ],
-        compiler_params=pltpu.CompilerParams(
-            collective_id=2, has_side_effects=True, vmem_limit_bytes=40 * 1024 * 1024
-        ),
-    )(outgoing, high, low, hidden, gate_weight, up_weight, down_weight)
-
-
-def on_device(
+def plain_on_device(
     residual,
     query_proj,
     key_proj,
@@ -436,10 +1058,6 @@
     )
     high = spread.astype(jnp.bfloat16)
     low = (spread - high.astype(jnp.float32)).astype(jnp.bfloat16)
-    if capacity % 16 == 0 and token_rows % capacity == 0 and experts_all % (token_rows // capacity) == 0:
-        return run_experts(
-            outgoing, high, low, hidden, gate_weight, up_weight, down_weight, capacity
-        )
     outgoing = outgoing.reshape(experts_all, capacity, normed.shape[1])
     arrived = lax.all_to_all(outgoing, ("sp", "tp"), split_axis=0, concat_axis=0, tiled=True)
     sources, slots, width = arrived.shape
@@ -462,6 +1080,32 @@
         low, rows_back, preferred_element_type=jnp.float32
     )
     return (hidden.astype(jnp.float32) + combined).astype(jnp.bfloat16)
+
+
+def on_device(*arrays):
+    (
+        residual, query_proj, key_proj, value_proj, query_gain, key_gain, document_ids,
+        output_weight, norm_gain, expert_ids, route_weights, gate_weight, up_weight, down_weight,
+    ) = arrays
+    token_rows = residual.shape[0]
+    top_count = expert_ids.shape[1]
+    experts_all = lax.axis_size("sp") * lax.axis_size("tp")
+    capacity = max(2, 2 * token_rows * top_count // experts_all)
+    if (
+        capacity % 16 == 0
+        and token_rows == HEAD
+        and token_rows % capacity == 0
+        and experts_all % (token_rows // capacity) == 0
+        and experts_all * capacity > 2 * token_rows
+        and 2 * top_count <= 8
+        and lax.axis_size("sp") % 2 == 0
+    ):
+        return run_layer(
+            query_proj, key_proj, value_proj, document_ids.reshape(1, -1), query_gain, key_gain,
+            expert_ids.T, route_weights.T, residual, norm_gain, output_weight,
+            gate_weight, up_weight, down_weight, capacity,
+        )
+    return plain_on_device(*arrays)
 
 
 def solution(mesh):

time: 165 us -> 128 us (0.78)
  Pallas kernels: 154 us -> 126 us
  other arithmetic: 4.03 us -> 0 us
  local copies, waits for them, and re-layouts: 5.71 us -> 1.88 us
    pallas_call x2 -> x1, Pallas kernels: 154 us -> 126 us  [run_layer(): pl.pallas_call(functools.partial(layer_kernel, n_sp, n_tp, capacity, top_...]
    unnamed x29 -> x1, local copies, waits for them, and re-layouts: 4.89 us -> 1.88 us
where the time goes in v2:
time: 128 us
  Pallas kernels  126 us (98%)
  local copies, waits for them, and re-layouts  1.88 us (1%)
    pallas_call x1, Pallas kernels, run_layer(): pl.pallas_call(functools.partial(layer_kernel, n_sp, n_tp, capacity, top_...  126 us

profile of v2, /device:TPU:0, one launch (start us, length us, event | category | flops | bytes accessed | tf_op | source)
XLA Modules:
  0.0 127.9 jit_solution(10575405575661142446)
XLA Ops:
  0.0 126.0 %shard_map.136 = bf16[128,2048]{1,0:T(8,128)(2,1)} custom-call(bf16[512,512]{1,0:T(8,128)(2,1)} %q_ref.1, bf16[512,128]{1,0:T(8,128)(2,1)} %k_ref.1, bf16[512,128]{1,0:T(8,128)(2,1)} %v_ref.1, s32[1,512]{1,0:T(1,128)} %bitcast.7, f32[1,128]{1,0:T(1,128)} %bitcast.10, f32[1,128]{1,0:T(1,128)} %bitcast.11, s32[2,128]{1,0:T(2,128)} %bitcast.8, ...), custom_call_target="tpu_custom_call" | custom-call | tf_op jit(solution)/shard_map/pallas_call | solution.py:707
  126.1 1.9 %copy.16 = bf16[128,2048]{1,0:T(8,128)(2,1)} copy(bf16[128,2048]{1,0:T(8,128)(2,1)} %shard_map.136) | data formatting | bytes 1048576

commit v3 on v2

--- a/solution.py
+++ b/solution.py
@@ -19,16 +19,19 @@
 MESH = pl.DeviceIdType.MESH
 DOC_KEY = 128.0
 DOC_QUERY = 64.0
-PIECES = 2
+PIECES = 4
+HALVES = 2
+LINE = 4
 OFFSETS = (1, -2, 2, -1, 3, -3)
 EXP2_SCALE = math.log2(math.e) / math.sqrt(HEAD)
 
 
 def layer_kernel(
     n_sp, n_tp, capacity, top_count,
-    q_ref, k_ref, v_ref, doc_ref, qg_ref, kg_ref, ids_ref, rw_ref, res_ref, gain_ref,
+    q_hbm, k_hbm, v_hbm, doc_hbm, qg_hbm, kg_hbm, ids_hbm, rw_hbm, res_hbm, gain_hbm,
     wo_hbm, gate_hbm, up_hbm, down_hbm,
     new_ref,
+    k_ref, v_ref, kg_ref, doc_ref, q_ref, qg_ref, ids_ref, rw_ref, res_ref, gain_ref,
     wo_v, gate_v, up_v, down_v, cos_s, sin_s, meta_s, q_aug, k_own, k_in, v_in, doc_in,
     k_aug, vt_s, m_s, l_s, acc_s, att_s, all_s, hid_s, nrm_s,
     metas, blocks, picked, arrived, answer, homing, returned, spread, total_s,
@@ -48,21 +51,29 @@
     plane = lax.div(me, members)
     pos = lax.rem(me, members)
 
-    loads = [
-        pltpu.make_async_copy(source.at[0], into, w_sem.at[i])
+    fetches = [
+        pltpu.make_async_copy(source, into, w_sem.at[i])
         for i, (source, into) in enumerate(
-            ((gate_hbm, gate_v), (up_hbm, up_v), (down_hbm, down_v))
+            (
+                (kg_hbm, kg_ref), (k_hbm, k_ref), (v_hbm, v_ref), (doc_hbm, doc_ref),
+                (ids_hbm, ids_ref), (rw_hbm, rw_ref), (qg_hbm, qg_ref), (q_hbm, q_ref),
+                (wo_hbm, wo_v), (res_hbm, res_ref), (gain_hbm, gain_ref),
+                (gate_hbm.at[0], gate_v), (up_hbm.at[0], up_v), (down_hbm.at[0], down_v),
+            )
         )
     ]
+    for fetch in fetches:
+        fetch.start()
+
+    def fetched(*which):
+        for i in which:
+            fetches[i].wait()
 
     def place(device):
         return (lax.div(device, n_tp), lax.rem(device, n_tp))
 
     def region(index):
         return pl.ds(pl.multiple_of(index * capacity, capacity), capacity)
-
-    def level(block):
-        return jnp.logical_and(block >= 0, block < groups)
 
     length = k_ref.shape[0]
     heads = q_ref.shape[1] // HEAD
@@ -87,11 +98,6 @@
     def reader(j):
         odd = OFFSETS[j] % 2 == 1
         return sp + side * OFFSETS[j] if odd else sp - side * OFFSETS[j]
-
-    wo_copy = pltpu.make_async_copy(wo_hbm, wo_v, w_sem.at[3])
-    wo_copy.start()
-    for load in loads:
-        load.start()
 
     barrier = pltpu.get_barrier_semaphore()
 
@@ -126,11 +132,23 @@
             [upper * cosine - lower * sine, upper * sine + lower * cosine], axis=0
         )
 
+    fetched(0, 1)
     k_own[...] = turned(k_ref[...], column(kg_ref[...])).T.astype(jnp.bfloat16)
+    fetched(2, 3, 4, 5)
     for k in range(top_count):
         for r, table in ((k, ids_ref), (top_count + k, rw_ref)):
             meta_s[r : r + 1, :] = table[k : k + 1, :].astype(jnp.float32)
     pl.semaphore_wait(barrier, devices - 1)
+
+    def tell(i, block):
+        return pltpu.make_async_remote_copy(
+            src_ref=meta_s,
+            dst_ref=metas.at[block],
+            send_sem=m_send.at[i],
+            recv_sem=m_recv.at[block],
+            device_id=place(lax.rem(plane + i, groups) * members + pos),
+            device_id_type=MESH,
+        )
 
     def shift(source, into, sends, receives, i, there):
         return pltpu.make_async_remote_copy(
@@ -193,7 +211,10 @@
         pl.when(inside(reader(j)))(lambda: doc_shift(j).start())
     start_keys(0, 1, 2)
     start_values(0, 1, 2)
-
+    for i in range(1, groups):
+        tell(i, plane).start()
+
+    fetched(6, 7)
     query_gains = column(qg_ref[...])
     for h in range(heads):
         q_aug[h, :HEAD, :] = turned(
@@ -276,50 +297,48 @@
         out = acc_s[h] / l_s[h]
         att_s[:, h * HEAD : (h + 1) * HEAD] = out.T.astype(jnp.bfloat16)
 
-    def exchange(k):
+    part_rows = rows // HALVES
+
+    def exchange(k, half):
         there = lax.rem(tp + k, n_tp)
+        here = pl.ds(pl.multiple_of(there * rows + half * part_rows, part_rows), part_rows)
         return pltpu.make_async_remote_copy(
-            src_ref=att_s.at[pl.ds(pl.multiple_of(there * rows, rows), rows), :],
-            dst_ref=all_s.at[tp],
-            send_sem=t_send.at[k],
-            recv_sem=t_recv.at[k],
+            src_ref=att_s.at[here, :],
+            dst_ref=all_s.at[tp, pl.ds(half * part_rows, part_rows)],
+            send_sem=t_send.at[k, half],
+            recv_sem=t_recv.at[k, half],
             device_id=(sp, there),
             device_id_type=MESH,
         )
 
-    for k in range(n_tp - 1, 0, -1):
-        exchange(k).start()
-    wo_copy.wait()
+    for half in range(HALVES):
+        for k in range(n_tp - 1, 0, -1):
+            exchange(k, half).start()
+    fetched(8, 9, 10)
 
     def weight_rows(i):
         return wo_v[pl.ds(pl.multiple_of(i * width, width), width), :]
 
-    projected = jnp.dot(
+    total_s[...] = res_ref[...].astype(jnp.float32) + jnp.dot(
         att_s[pl.ds(pl.multiple_of(tp * rows, rows), rows), :],
         weight_rows(tp),
         preferred_element_type=jnp.float32,
     )
-    for k in range(1, n_tp):
-        exchange(k).wait_recv()
-        source = lax.rem(tp - k + n_tp, n_tp)
-        projected += jnp.dot(
-            all_s[source], weight_rows(source), preferred_element_type=jnp.float32
-        )
-    hidden = (res_ref[...].astype(jnp.float32) + projected).astype(jnp.bfloat16)
-    hid_s[...] = hidden
-    wide = hidden.astype(jnp.float32)
-    mean = jnp.mean(wide * wide, axis=-1, keepdims=True)
-    nrm_s[...] = (wide * lax.rsqrt(mean + norm_eps) * gain_ref[...]).astype(jnp.bfloat16)
-
-    def tell(i, block):
-        return pltpu.make_async_remote_copy(
-            src_ref=meta_s,
-            dst_ref=metas.at[block],
-            send_sem=m_send.at[i],
-            recv_sem=m_recv.at[block],
-            device_id=place(lax.rem(plane + i, groups) * members + pos),
-            device_id_type=MESH,
-        )
+
+    def project(half):
+        part = pl.ds(half * part_rows, part_rows)
+        projected = total_s[part, :]
+        for k in range(1, n_tp):
+            exchange(k, half).wait_recv()
+            source = lax.rem(tp - k + n_tp, n_tp)
+            projected += jnp.dot(
+                all_s[source, part, :], weight_rows(source), preferred_element_type=jnp.float32
+            )
+        hidden = projected.astype(jnp.bfloat16)
+        hid_s[part, :] = hidden
+        wide = hidden.astype(jnp.float32)
+        mean = jnp.mean(wide * wide, axis=-1, keepdims=True)
+        nrm_s[part, :] = (wide * lax.rsqrt(mean + norm_eps) * gain_ref[...]).astype(jnp.bfloat16)
 
     def pass_on(source, block, way, c):
         part = pl.ds(c * piece, piece)
@@ -402,14 +421,44 @@
 
         lax.fori_loop(first, members, one, 0)
 
-    for i in range(1, groups):
-        tell(i, plane).start()
-    for way in range(2):
-
-        @pl.when(level(plane + 2 * way - 1))
+    low_side = plane < groups // 2
+    toward = jnp.where(low_side, 1, -1)
+    seen = jnp.where(low_side, 0, 1)
+    inward, outward = 1 - seen, seen
+    is_end = jnp.logical_or(plane == 0, plane == groups - 1)
+    is_inner = jnp.logical_not(is_end)
+    first = jnp.where(is_end, plane + toward, plane - toward)
+    second = jnp.where(is_end, plane + 3 * toward, plane + 2 * toward)
+    third = jnp.where(is_end, plane + 2 * toward, plane + toward)
+    early, late = range(PIECES // 2), range(PIECES // 2, PIECES)
+
+    def push(source, block, way, which):
+        for c in which:
+            pass_on(source, block, way, c).start()
+
+    def landed(block, which):
+        for c in which:
+            pass_on(nrm_s, block, 0, c).wait_recv()
+
+    def hop(block, way, which):
+        for c in which:
+            landed(block, (c,))
+            push(blocks.at[block], block, way, (c,))
+
+    for half in range(HALVES):
+        project(half)
+        ready = range(half * PIECES // HALVES, (half + 1) * PIECES // HALVES)
+
+        @pl.when(is_end)
         def _():
-            for c in range(PIECES):
-                pass_on(nrm_s, plane, way, c).start()
+            push(nrm_s, plane, inward, ready)
+
+        @pl.when(is_inner)
+        def _():
+            for c in ready:
+                push(nrm_s, plane, outward, (c,))
+                if c in early:
+                    push(nrm_s, plane, inward, (c,))
 
     def slot_rows(meta):
         experts = lax.broadcasted_iota(jnp.int32, (devices, rows), 0).astype(jnp.float32)
@@ -453,18 +502,6 @@
         answer[block] = jnp.dot(
             activity, down_v[...], preferred_element_type=jnp.float32
         ).astype(jnp.bfloat16)
-
-    def both_ways(distance, act):
-        def one(way, carry):
-            block = plane - (2 * way - 1) * distance
-
-            @pl.when(level(block))
-            def _():
-                act(block, way)
-
-            return carry
-
-        lax.fori_loop(0, 2, one, 0)
 
     gather(nrm_s, meta_s[...], plane)
     own_slots = slot_rows(meta_s[...])
@@ -477,48 +514,21 @@
         high = weights.astype(jnp.bfloat16)
         spread[g, 0] = high
         spread[g, 1] = (weights - high.astype(jnp.float32)).astype(jnp.bfloat16)
-    for load in loads:
-        load.wait()
-
-    def receive(block, way, c):
-        pass_on(nrm_s, block, way, c).wait_recv()
-
-        @pl.when(level(plane + 2 * way - 1))
-        def _():
-            pass_on(blocks.at[block], block, way, c).start()
-
-    def collect(block, way):
+    fetched(11, 12, 13)
+
+    def collect(block):
         tell(1, block).wait_recv()
         gather(blocks.at[block], metas[block], block)
 
-    def beyond(way):
-        return level(plane - (1 - 2 * way))
-
-    def past(block, way):
-        return level(block + (1 - 2 * way))
-
-    def relayed(distance, far):
-        return far if distance == 2 else distance == 3
-
-    def serve(block, way, distance):
+    def serve_home(block):
         expert(block)
-        joint = relayed(distance, beyond(way))
-
-        def raw():
-            for c in range(PIECES):
-                give_home(block, plane, c).start()
-
-        def through():
-            others(lambda member: give_across(block, member, pos).start())
-            back[block, region(pos), :] = answer[block, region(pos), :]
-
-        if joint is True:
-            through()
-        elif joint is False:
-            raw()
-        else:
-            pl.when(joint)(through)
-            pl.when(jnp.logical_not(joint))(raw)
+        for c in range(PIECES):
+            give_home(block, plane, c).start()
+
+    def serve_across(block):
+        expert(block)
+        others(lambda member: give_across(block, member, pos).start())
+        back[block, region(pos), :] = answer[block, region(pos), :]
 
     def join(block):
         others(lambda member: give_across(block, member, member).wait_recv())
@@ -536,68 +546,83 @@
             + jnp.dot(low, back[block], preferred_element_type=jnp.float32)
         ).astype(jnp.bfloat16)
 
-    def begin_chain(block, way):
-        join(block)
+    def share(origin):
         for c in range(PIECES):
-            give_next(block, way, c).start()
-
-    def extend_chain(block, way):
-        @pl.when(beyond(way))
-        def _():
-            join(block)
-            for c in range(PIECES):
-                part = pl.ds(c * piece, piece)
-                give_next(block, way, c).wait_recv()
-                joined[block, part, :] = (
-                    joined[block, part, :].astype(jnp.float32)
-                    + midway[way, part, :].astype(jnp.float32)
-                ).astype(jnp.bfloat16)
-                give_sum(block, way, c).start()
-
-    def serve_at(distance):
-        both_ways(distance, functools.partial(serve, distance=distance))
-
-    def share(origin, way, distance):
-        def pieces():
-            for c in range(PIECES):
-                give_home(origin, origin, c).wait_recv()
-                for i in range(c * members // PIECES, (c + 1) * members // PIECES):
-
-                    @pl.when(pos != i)
-                    def _():
-                        give_back(homing.at[origin], origin, i, pos).start()
-
-            returned[region(origin * members + pos), :] = homing[origin, region(pos), :]
-
-        on(raw_from(origin, way, distance), pieces)
-
-    def raw_from(origin, way, distance):
-        joint = relayed(distance, level(origin - (2 * way - 1)))
-        return not joint if isinstance(joint, bool) else jnp.logical_not(joint)
-
-    def share_at(distance):
-        if distance != 3:
-            both_ways(distance, functools.partial(share, distance=distance))
-
-    for distance in range(1, groups):
+            give_home(origin, origin, c).wait_recv()
+            for i in range(c * members // PIECES, (c + 1) * members // PIECES):
+
+                @pl.when(pos != i)
+                def _():
+                    give_back(homing.at[origin], origin, i, pos).start()
+
+        returned[region(origin * members + pos), :] = homing[origin, region(pos), :]
+
+    @pl.when(is_inner)
+    def _():
+        hop(first, inward, range(PIECES - 1))
+        hop(second, outward, (0,))
+        hop(first, inward, (PIECES - 1,))
+        push(nrm_s, plane, inward, late)
+        hop(second, outward, (1,))
+
+    @pl.when(is_end)
+    def _():
+        landed(first, range(PIECES))
+
+    collect(first)
+    expert(plane)
+    others(lambda member: give_back(answer.at[plane], plane, member, pos).start())
+    returned[region(me), :] = answer[plane, region(pos), :]
+
+    @pl.when(is_inner)
+    def _():
+        hop(second, outward, range(2, PIECES))
+        hop(third, outward, early)
+
+    @pl.when(is_end)
+    def _():
+        landed(second, range(PIECES))
+
+    collect(second)
+    serve_home(first)
+
+    @pl.when(is_end)
+    def _():
+        serve_across(second)
+        landed(third, range(PIECES))
+
+    @pl.when(is_inner)
+    def _():
+        hop(third, outward, late)
+
+    collect(third)
+
+    @pl.when(is_inner)
+    def _():
+        serve_across(second)
+
+    @pl.when(is_end)
+    def _():
+        join(second)
         for c in range(PIECES):
-            if c == PIECES - 1:
-                if distance == 1:
-                    expert(plane)
-                    others(lambda member: give_back(answer.at[plane], plane, member, pos).start())
-                    returned[region(me), :] = answer[plane, region(pos), :]
-                else:
-                    serve_at(distance - 1)
-            both_ways(distance, functools.partial(receive, c=c))
-        both_ways(distance, collect)
-        if distance > 2:
-            share_at(distance - 2)
-    serve_at(groups - 1)
-    if groups > 3:
-        both_ways(3, begin_chain)
-    share_at(max(1, groups - 2))
-    both_ways(2, extend_chain)
-    share_at(groups - 1)
+            give_next(second, seen, c).start()
+
+    serve_home(third)
+    share(first)
+
+    @pl.when(is_inner)
+    def _():
+        join(second)
+        for c in range(PIECES):
+            part = pl.ds(c * piece, piece)
+            give_next(second, seen, c).wait_recv()
+            joined[second, part, :] = (
+                joined[second, part, :].astype(jnp.float32)
+                + midway[seen, part, :].astype(jnp.float32)
+            ).astype(jnp.bfloat16)
+            give_sum(second, seen, c).start()
+        share(third)
+        share(second)
 
     total = hid_s[...].astype(jnp.float32)
 
@@ -610,72 +635,53 @@
         others(lambda member: give_back(homing.at[origin], origin, member, member).wait_recv())
         return combine(origin)
 
-    total_s[...] = total + gathered(plane)
-
-    def add(origin, way, distance):
-        def slots_back():
-            total_s[...] += gathered(origin)
-
-        def sum_back():
-            for c in range(PIECES):
-                give_sum(origin, 1 - way, c).wait_recv()
-            total_s[...] += summed[1 - way].astype(jnp.float32)
-
-        raw = raw_from(origin, way, distance)
-        on(raw, slots_back)
-        if distance == 2:
-            pl.when(jnp.logical_not(raw))(sum_back)
-
-    for distance in range(1, groups):
-        if distance != 3:
-            both_ways(distance, functools.partial(add, distance=distance))
+    total_s[...] = total + gathered(plane) + gathered(first)
+
+    @pl.when(is_inner)
+    def _():
+        total_s[...] += gathered(third)
+        total_s[...] += gathered(second)
+
+    @pl.when(is_end)
+    def _():
+        for c in range(PIECES):
+            give_sum(third, 1 - seen, c).wait_recv()
+        total_s[...] += summed[1 - seen].astype(jnp.float32)
+
     new_ref[...] = total_s[...].astype(jnp.bfloat16)
 
     for i in range(1, groups):
         tell(i, plane).wait_send()
-    for way in range(2):
-
-        @pl.when(level(plane + 2 * way - 1))
-        def _():
-            for c in range(PIECES):
-                pass_on(nrm_s, plane, way, c).wait_send()
-
-    def sent(block, way, distance):
-        @pl.when(level(plane + 2 * way - 1))
-        def _():
-            for c in range(PIECES):
-                pass_on(nrm_s, block, way, c).wait_send()
-
-        others(lambda peer: dispatch(block, peer, pos).wait_send())
-
-        def shared():
-            others(lambda member: give_back(homing.at[block], block, member, pos).wait_send())
-
-        def raw():
-            for c in range(PIECES):
-                give_home(block, plane, c).wait_send()
-
-        def through():
-            others(lambda member: give_across(block, member, pos).wait_send())
-            for c in range(PIECES):
-                give_next(block, way, c).wait_send()
-
-        if distance != 3:
-            on(raw_from(block, way, distance), shared)
-        joint = relayed(distance, beyond(way))
-        if joint is True:
-            through()
-        elif joint is False:
-            raw()
-        else:
-            pl.when(joint)(through)
-            pl.when(jnp.logical_not(joint))(raw)
+
+    def gone(block, way):
+        for c in range(PIECES):
+            pass_on(nrm_s, block, way, c).wait_send()
+
+    gone(plane, inward)
+
+    @pl.when(is_inner)
+    def _():
+        gone(plane, outward)
+        gone(first, inward)
+        gone(second, outward)
+        gone(third, outward)
 
     others(lambda peer: dispatch(plane, peer, pos).wait_send())
     others(lambda member: give_back(answer.at[plane], plane, member, pos).wait_send())
-    for distance in range(1, groups):
-        both_ways(distance, functools.partial(sent, distance=distance))
-
+    for block in (first, second, third):
+        others(lambda peer: dispatch(block, peer, pos).wait_send())
+    for block in (first, third):
+        for c in range(PIECES):
+            give_home(block, plane, c).wait_send()
+    others(lambda member: give_across(second, member, pos).wait_send())
+    for c in range(PIECES):
+        give_next(second, seen, c).wait_send()
+    others(lambda member: give_back(homing.at[first], first, member, pos).wait_send())
+
+    @pl.when(is_inner)
+    def _():
+        for block in (second, third):
+            others(lambda member: give_back(homing.at[block], block, member, pos).wait_send())
 
     for i in range(slots):
         on(key_plan[i][2], lambda: key_shift(i).wait_send())
@@ -683,7 +689,8 @@
     for i in range(slots + 1):
         on(value_plan[i][2], lambda: value_shift(i).wait_send())
     for k in range(1, n_tp):
-        exchange(k).wait_send()
+        for half in range(HALVES):
+            exchange(k, half).wait_send()
 
 
 def run_layer(
@@ -701,15 +708,24 @@
     block = (length, HEAD)
     narrow = jnp.bfloat16
     vmem = pl.BlockSpec(memory_space=pltpu.VMEM)
-    anywhere = pl.BlockSpec(memory_space=pl.ANY)
     buffer = pltpu.VMEM((groups, rows, model), narrow)
     dma = pltpu.SemaphoreType.DMA
     return pl.pallas_call(
         functools.partial(layer_kernel, n_sp, n_tp, capacity, top_count),
         out_shape=jax.ShapeDtypeStruct(residual.shape, narrow),
-        in_specs=[vmem] * 10 + [anywhere] * 4,
+        in_specs=[pl.BlockSpec(memory_space=pltpu.HBM)] * 14,
         out_specs=vmem,
         scratch_shapes=[
+            pltpu.VMEM(block, narrow),
+            pltpu.VMEM(block, narrow),
+            pltpu.VMEM((1, HEAD), jnp.float32),
+            pltpu.VMEM(docs.shape, jnp.int32),
+            pltpu.VMEM(query_proj.shape, narrow),
+            pltpu.VMEM((1, HEAD), jnp.float32),
+            pltpu.VMEM(expert_ids.shape, jnp.int32),
+            pltpu.VMEM(route_weights.shape, jnp.float32),
+            pltpu.VMEM(residual.shape, narrow),
+            pltpu.VMEM((1, model), jnp.float32),
             pltpu.VMEM(output_weight.shape, narrow),
             pltpu.VMEM(gate_weight.shape[1:], narrow),
             pltpu.VMEM(up_weight.shape[1:], narrow),
@@ -750,8 +766,8 @@
             dma((slots + 1,)),
             dma((slots,)),
             dma((slots,)),
-            dma((n_tp,)),
-            dma((n_tp,)),
+            dma((n_tp, HALVES)),
+            dma((n_tp, HALVES)),
             dma((groups,)),
             dma((groups,)),
             dma((2, groups, PIECES)),
@@ -767,7 +783,7 @@
             dma((groups, PIECES)),
             dma((2, PIECES)),
             dma((2, PIECES)),
-            dma((4,)),
+            dma((14,)),
         ],
         compiler_params=pltpu.CompilerParams(
             collective_id=1, has_side_effects=True, vmem_limit_bytes=60 * 1024 * 1024
@@ -1096,7 +1112,7 @@
         and token_rows == HEAD
         and token_rows % capacity == 0
         and experts_all % (token_rows // capacity) == 0
-        and experts_all * capacity > 2 * token_rows
+        and experts_all * capacity == LINE * token_rows
         and 2 * top_count <= 8
         and lax.axis_size("sp") % 2 == 0
     ):

time: 128 us -> 116 us (0.906)
  Pallas kernels: 126 us -> 114 us
    pallas_call x1, Pallas kernels: 126 us -> 114 us  [run_layer(): pl.pallas_call(functools.partial(layer_kernel, n_sp, n_tp, capacity, top_...]
where the time goes in v3:
time: 116 us
  Pallas kernels  114 us (98%)
  local copies, waits for them, and re-layouts  1.88 us (2%)
    pallas_call x1, Pallas kernels, run_layer(): pl.pallas_call(functools.partial(layer_kernel, n_sp, n_tp, capacity, top_...  114 us

profile of v3, /device:TPU:0, one launch (start us, length us, event | category | flops | bytes accessed | tf_op | source)
XLA Modules:
  0.0 116.3 jit_solution(8340276480974035154)
XLA Ops:
  0.0 114.4 %shard_map.136 = bf16[128,2048]{1,0:T(8,128)(2,1)} custom-call(bf16[512,512]{1,0:T(8,128)(2,1)} %q_hbm.1, bf16[512,128]{1,0:T(8,128)(2,1)} %k_hbm.1, bf16[512,128]{1,0:T(8,128)(2,1)} %v_hbm.1, s32[1,512]{1,0:T(1,128)} %bitcast.7, f32[1,128]{1,0:T(1,128)} %bitcast.10, f32[1,128]{1,0:T(1,128)} %bitcast.11, s32[2,128]{1,0:T(2,128)} %bitcast.8, ...), custom_call_target="tpu_custom_call" | custom-call | tf_op jit(solution)/shard_map/pallas_call | solution.py:713
  114.4 1.9 %copy.16 = bf16[128,2048]{1,0:T(8,128)(2,1)} copy(bf16[128,2048]{1,0:T(8,128)(2,1)} %shard_map.136) | data formatting | bytes 1048576

commit v4 on v3

--- a/solution.py
+++ b/solution.py
@@ -20,6 +20,8 @@
 DOC_KEY = 128.0
 DOC_QUERY = 64.0
 PIECES = 4
+ONES = 16
+DOC_MARK = 32.0
 HALVES = 2
 LINE = 4
 OFFSETS = (1, -2, 2, -1, 3, -3)
@@ -33,7 +35,7 @@
     new_ref,
     k_ref, v_ref, kg_ref, doc_ref, q_ref, qg_ref, ids_ref, rw_ref, res_ref, gain_ref,
     wo_v, gate_v, up_v, down_v, cos_s, sin_s, meta_s, q_aug, k_own, k_in, v_in, doc_in,
-    k_aug, vt_s, m_s, l_s, acc_s, att_s, all_s, hid_s, nrm_s,
+    k_aug, vt_s, m_s, acc_s, att_s, all_s, hid_s, nrm_s,
     metas, blocks, picked, arrived, answer, homing, returned, spread, total_s,
     back, joined, midway, summed,
     k_send, k_recv, v_send, v_recv, c_send, c_recv, t_send, t_recv,
@@ -215,13 +217,13 @@
         tell(i, plane).start()
 
     fetched(6, 7)
-    query_gains = column(qg_ref[...])
+    query_gains = column(qg_ref[...]) * EXP2_SCALE
     for h in range(heads):
         q_aug[h, :HEAD, :] = turned(
             q_ref[:, h * HEAD : (h + 1) * HEAD], query_gains
         ).astype(jnp.bfloat16)
         labels = lax.broadcasted_iota(jnp.int32, (HEAD, length), 0)
-        q_aug[h, HEAD:, :] = jnp.where(doc_ref[...] == labels, DOC_QUERY, 0.0).astype(
+        q_aug[h, HEAD:, :] = jnp.where(doc_ref[...] == labels, DOC_MARK, 0.0).astype(
             jnp.bfloat16
         )
 
@@ -229,27 +231,19 @@
         doc_col = jnp.broadcast_to(docs[...].astype(jnp.float32), (HEAD, length)).T
         lanes = lax.broadcasted_iota(jnp.int32, (length, HEAD), 1).astype(jnp.float32)
         k_aug[:, :HEAD] = keys[...]
-        k_aug[:, HEAD:] = jnp.where(doc_col == lanes, DOC_KEY, 0.0).astype(jnp.bfloat16)
-        vt_s[...] = values[...].T
+        k_aug[:, HEAD:] = jnp.where(doc_col == lanes, DOC_MARK, 0.0).astype(jnp.bfloat16)
+        vt_s[:HEAD, :] = values[...].T
         for h in range(heads):
             s = jnp.dot(k_aug[...], q_aug[h], preferred_element_type=jnp.float32)
             top = jnp.max(s, axis=0, keepdims=True)
             if not first:
                 top = jnp.maximum(m_s[h], top)
-            e = jnp.exp2((s - top) * EXP2_SCALE)
-            den = jnp.sum(e, axis=0, keepdims=True)
-            part = jnp.dot(
-                vt_s[...], e.astype(jnp.bfloat16), preferred_element_type=jnp.float32
-            )
-            if first:
-                l_s[h] = den
-                acc_s[h] = part
-            else:
-                old = jnp.exp2((m_s[h] - top) * EXP2_SCALE)
-                l_s[h] = l_s[h] * old + den
-                acc_s[h] = acc_s[h] * old + part
+            e = jnp.exp2(s - top).astype(jnp.bfloat16)
+            part = jnp.dot(vt_s[...], e, preferred_element_type=jnp.float32)
+            acc_s[h] = part if first else acc_s[h] * jnp.exp2(m_s[h] - top) + part
             m_s[h] = top
 
+    vt_s[HEAD:, :] = jnp.ones((ONES, length), jnp.bfloat16)
     take(k_own, v_ref, doc_ref, True)
 
     key_wait(0)
@@ -294,7 +288,7 @@
     lax.fori_loop(0, slots, step, 0)
 
     for h in range(heads):
-        out = acc_s[h] / l_s[h]
+        out = acc_s[h, :HEAD, :] / acc_s[h, HEAD : HEAD + 1, :]
         att_s[:, h * HEAD : (h + 1) * HEAD] = out.T.astype(jnp.bfloat16)
 
     part_rows = rows // HALVES
@@ -590,22 +584,19 @@
     def _():
         serve_across(second)
         landed(third, range(PIECES))
-
-    @pl.when(is_inner)
-    def _():
-        hop(third, outward, late)
-
-    collect(third)
-
-    @pl.when(is_inner)
-    def _():
-        serve_across(second)
-
-    @pl.when(is_end)
-    def _():
         join(second)
         for c in range(PIECES):
             give_next(second, seen, c).start()
+
+    @pl.when(is_inner)
+    def _():
+        hop(third, outward, late)
+
+    collect(third)
+
+    @pl.when(is_inner)
+    def _():
+        serve_across(second)
 
     serve_home(third)
     share(first)
@@ -739,10 +730,9 @@
             pltpu.VMEM((slots + 1,) + block, narrow),
             pltpu.VMEM((slots,) + docs.shape, jnp.int32),
             pltpu.VMEM((length, 2 * HEAD), narrow),
-            pltpu.VMEM((HEAD, length), narrow),
+            pltpu.VMEM((HEAD + ONES, length), narrow),
             pltpu.VMEM((heads, 1, length), jnp.float32),
-            pltpu.VMEM((heads, 1, length), jnp.float32),
-            pltpu.VMEM((heads, HEAD, length), jnp.float32),
+            pltpu.VMEM((heads, HEAD + ONES, length), jnp.float32),
             pltpu.VMEM((length, heads * HEAD), narrow),
             pltpu.VMEM((n_tp, rows, heads * HEAD), narrow),
             pltpu.VMEM((rows, model), narrow),

time: 116 us -> 115 us (level)
    pallas_call x1, Pallas kernels: 114 us -> 113 us  [run_layer(): pl.pallas_call(functools.partial(layer_kernel, n_sp, n_tp, capacity, top_...]
where the time goes in v4:
time: 115 us
  Pallas kernels  113 us (98%)
  local copies, waits for them, and re-layouts  1.88 us (2%)
    pallas_call x1, Pallas kernels, run_layer(): pl.pallas_call(functools.partial(layer_kernel, n_sp, n_tp, capacity, top_...  113 us

profile of v4, /device:TPU:0, one launch (start us, length us, event | category | flops | bytes accessed | tf_op | source)
XLA Modules:
  0.0 115.0 jit_solution(12093248399571675238)
XLA Ops:
  0.0 113.1 %shard_map.136 = bf16[128,2048]{1,0:T(8,128)(2,1)} custom-call(bf16[512,512]{1,0:T(8,128)(2,1)} %q_hbm.1, bf16[512,128]{1,0:T(8,128)(2,1)} %k_hbm.1, bf16[512,128]{1,0:T(8,128)(2,1)} %v_hbm.1, s32[1,512]{1,0:T(1,128)} %bitcast.7, f32[1,128]{1,0:T(1,128)} %bitcast.10, f32[1,128]{1,0:T(1,128)} %bitcast.11, s32[2,128]{1,0:T(2,128)} %bitcast.8, ...), custom_call_target="tpu_custom_call" | custom-call | tf_op jit(solution)/shard_map/pallas_call | solution.py:704
  113.1 1.9 %copy.16 = bf16[128,2048]{1,0:T(8,128)(2,1)} copy(bf16[128,2048]{1,0:T(8,128)(2,1)} %shard_map.136) | data formatting | bytes 1048576

commit v5 on v4

--- a/solution.py
+++ b/solution.py
@@ -587,6 +587,7 @@
         join(second)
         for c in range(PIECES):
             give_next(second, seen, c).start()
+        share(first)
 
     @pl.when(is_inner)
     def _():
@@ -599,10 +600,10 @@
         serve_across(second)
 
     serve_home(third)
-    share(first)
 
     @pl.when(is_inner)
     def _():
+        share(first)
         join(second)
         for c in range(PIECES):
             part = pl.ds(c * piece, piece)

time: 115 us -> 118 us (1.026)
  the two profiles are of different devices: /device:TPU:0 before, /device:TPU:15 now
where the time goes in v5:
time: 118 us
  Pallas kernels  116 us (98%)
  local copies, waits for them, and re-layouts  1.88 us (2%)
    pallas_call x1, Pallas kernels, run_layer(): pl.pallas_call(functools.partial(layer_kernel, n_sp, n_tp, capacity, top_...  116 us

profile of v5, /device:TPU:15, one launch (start us, length us, event | category | flops | bytes accessed | tf_op | source)
XLA Modules:
  0.0 117.8 jit_solution(4160615631951557320)
XLA Ops:
  0.0 115.9 %shard_map.136 = bf16[128,2048]{1,0:T(8,128)(2,1)} custom-call(bf16[512,512]{1,0:T(8,128)(2,1)} %q_hbm.1, bf16[512,128]{1,0:T(8,128)(2,1)} %k_hbm.1, bf16[512,128]{1,0:T(8,128)(2,1)} %v_hbm.1, s32[1,512]{1,0:T(1,128)} %bitcast.7, f32[1,128]{1,0:T(1,128)} %bitcast.10, f32[1,128]{1,0:T(1,128)} %bitcast.11, s32[2,128]{1,0:T(2,128)} %bitcast.8, ...), custom_call_target="tpu_custom_call" | custom-call | tf_op jit(solution)/shard_map/pallas_call | solution.py:705
  115.9 1.9 %copy.16 = bf16[128,2048]{1,0:T(8,128)(2,1)} copy(bf16[128,2048]{1,0:T(8,128)(2,1)} %shard_map.136) | data formatting | bytes 1048576
